TPU v7x, 128 devices: a whole 4x4x4 slice. The times are simulated.
128 devices in a mesh: ep: 16 (over z, x), tp: 8 (over y, core).
Axes of the slice: x: 4, y: 4, z: 4, core: 2. Of those that a mesh axis runs over, the one named last changes fastest.
Arguments:
- queries: bfloat16 [32768, 512], P('ep', 'tp'), may hold values from -6 to 6
- head_key_rows: bfloat16 [32768, 512], P('ep', 'tp'), may hold values from -6 to 6
- head_value_rows: bfloat16 [32768, 1024], P('ep', 'tp'), may hold values from -18 to 18
- log_input_gate: float32 [32768, 8], P('ep', 'tp'), may hold values from -6 to 120
- forget_logits: float32 [32768, 8], P('ep', 'tp'), may hold values from -8 to 8
- head_forget_bias: float32 [8], P('tp'), may hold values from 3 to 20
- extra_log_forget: float32 [32768, 8], P('ep', 'tp'), may hold values from -1 to 0
- output_gate_logits: bfloat16 [32768, 1024], P('ep', 'tp'), may hold values from -6 to 6
- head_norm_gain: float32 [1024], P('tp'), may hold values from 0.1 to 1.9
- mixer_output_weight: bfloat16 [1024, 2048], replicated, may hold values from -0.1875 to 0.1875
- second_batch_input: bfloat16 [24576, 2048], P(('ep', 'tp')), may hold values from -6 to 6
- expert_norm_gain: float32 [2048], replicated, may hold values from 0.1 to 1.9
- routed_expert_index: int32 [24576, 2], P(('ep', 'tp')), may hold values from 0 to 127, all different within a row; in each aligned block of 192 rows (0 to 191, 192 to 383, ...) at most 4 rows name the same one
- routed_copy_weight: float32 [24576, 2], P(('ep', 'tp')), may hold values from 0.3 to 1.5
- routed_gate_weight: bfloat16 [128, 2048, 1024], P(('ep', 'tp')), may hold values from -0.125 to 0.125
- routed_up_weight: bfloat16 [128, 2048, 1024], P(('ep', 'tp')), may hold values from -0.125 to 0.125
- routed_down_weight: bfloat16 [128, 1024, 2048], P(('ep', 'tp')), may hold values from -0.1875 to 0.1875
- shared_gate_weight: bfloat16 [2048, 384], replicated, may hold values from -0.125 to 0.125
- shared_up_weight: bfloat16 [2048, 384], replicated, may hold values from -0.125 to 0.125
- shared_down_weight: bfloat16 [384, 2048], replicated, may hold values from -0.3125 to 0.3125
Outputs:
- mixer_first_output: bfloat16 [32768, 2048], P(('ep', 'tp'))
- moe_out: bfloat16 [24576, 2048], P(('ep', 'tp'))
Inputs may be any that keep to these rules, and one draw needn't show every extreme that they name: `routed_expert_index`: in each aligned block of 192 rows (the rows of one device) no expert is named by more than 4 rows, and in some blocks one expert is named by exactly 4; every expert is named somewhere.
All inputs are finite; a program needn't handle non-finite values.
Results may differ from a plain program's by a relative error of at most 0.0068.
Values may be sent and summed in bfloat16 or wider, within the bound.
No kernel may reach another device: no remote copies, remote signals or barrier semaphores. Data moves between devices by JAX's collectives and lax.ppermute only.
A program may use at most 128 MiB of HBM per device.

v0:
```python
import jax
import jax.numpy as jnp
from jax import lax
from jax.experimental import pallas as pl
from jax.experimental.pallas import tpu as pltpu
from jax.sharding import Mesh
from jax.sharding import PartitionSpec as P


EP = ("ep_0", "ep_1")
EP_TP = ("ep_0", "ep_1", "tp")
BLK = 128
F32 = jnp.float32
BF16 = jnp.bfloat16
NEG = -1e30


def split_two(x):
    hi = x.astype(BF16)
    return hi, (x - hi.astype(F32)).astype(BF16)


def dot(a, b, dims=(((1,), (0,)), ((), ()))):
    return lax.dot_general(a, b, dims, preferred_element_type=F32)


def exact_dot(a, b, dims=(((1,), (0,)), ((), ()))):
    return lax.dot_general(
        a, b, dims, precision=lax.Precision.HIGHEST, preferred_element_type=F32
    )


def iota(shape, dim):
    return lax.broadcasted_iota(jnp.int32, shape, dim)


def whole(shape):
    return pl.BlockSpec(shape, lambda *_: (0,) * len(shape))


def params(mib, grid=False):
    return pltpu.CompilerParams(
        vmem_limit_bytes=mib * 2**20,
        dimension_semantics=("arbitrary",) if grid else None,
    )


def in_hbm(*arrays):
    return [pltpu.with_memory_space_constraint(a, pltpu.HBM) for a in arrays]


def cost(flops, nbytes):
    return pl.CostEstimate(flops=int(flops), bytes_accessed=int(nbytes), transcendentals=0)


def slot_rows(idx, cap, experts):
    tokens = idx.shape[1]
    sub = iota((experts, tokens), 0)
    first = sub == idx[0:1, :]
    second = sub == idx[1:2, :]
    named = jnp.where(first | second, 1.0, 0.0).astype(BF16)
    before = jnp.where(iota((tokens, tokens), 0) < iota((tokens, tokens), 1), 1.0, 0.0)
    prior = dot(named, before.astype(BF16))
    places = [jnp.sum(jnp.where(hot, prior, 0.0), axis=0, keepdims=True) for hot in (first, second)]
    return [
        idx[j : j + 1, :] * (2 * cap) + places[j].astype(jnp.int32) for j in range(2)
    ]


def dispatch_body(cap, experts, x_ref, gain_ref, idx_ref, send_ref, normed_ref, rows_ref, both_ref, want_ref):
    step = pl.program_id(0)
    tokens, width = x_ref.shape
    half = width // 2

    @pl.when(step == 0)
    def _():
        x = x_ref[...].astype(F32)
        scale = lax.rsqrt(jnp.mean(x * x, axis=-1, keepdims=True) + 1e-06)
        normed = (x * scale * gain_ref[...]).astype(BF16)
        normed_ref[...] = normed
        both_ref[0:tokens, :] = normed[:, :half]
        both_ref[tokens:, :] = normed[:, half:]
        row0, row1 = slot_rows(idx_ref[...], cap, experts)
        rows_ref[...] = jnp.concatenate([row0, row1, row0, row1, row0, row1, row0, row1], axis=0)
        want_ref[0:1, 0:tokens] = row0
        want_ref[1:2, 0:tokens] = row1

    rows = send_ref.shape[0]
    row = iota((rows, tokens), 0) + step * rows
    t0, t1 = want_ref[0:1, 0:tokens], want_ref[1:2, 0:tokens]
    low = jnp.where((row == t0) | (row == t1), 1.0, 0.0).astype(BF16)
    high = jnp.where((row == t0 + cap) | (row == t1 + cap), 1.0, 0.0).astype(BF16)
    out = dot(low, both_ref[0:tokens, :]) + dot(high, both_ref[tokens:, :])
    send_ref[...] = out.astype(BF16)


def dispatch_rows(x, gain, idx, cap, experts):
    tokens, width = x.shape
    total = experts * cap * 2
    steps = 4
    body = lambda *refs: dispatch_body(cap, experts, *refs)
    return pl.pallas_call(
        body,
        grid=(steps,),
        in_specs=[whole((tokens, width)), whole((1, width)), whole((2, tokens))],
        out_specs=[
            pl.BlockSpec((total // steps, width // 2), lambda i: (i, 0)),
            whole((tokens, width)),
            whole((8, tokens)),
        ],
        out_shape=[
            pltpu.HBM((total, width // 2), BF16),
            pltpu.HBM((tokens, width), BF16),
            pltpu.HBM((8, tokens), jnp.int32),
        ],
        scratch_shapes=[pltpu.VMEM((2 * tokens, width // 2), BF16), pltpu.VMEM((8, 256), jnp.int32)],
        compiler_params=params(20, True),
        cost_estimate=cost(2 * total * tokens * width, 4 * total * width),
        name="dispatch_rows",
    )(*in_hbm(x, gain, idx))


def swap_halves(even, odd, lower):
    first = jnp.where(lower, even, pltpu.roll(odd, 4, 1))
    last = jnp.where(lower, pltpu.roll(even, 4, 1), odd)
    return first, last


def expert_body(pieces, a_ref, g_hbm, u_hbm, d_hbm, out_hbm, x_ref, h_ref, g_ref, u_ref, d_ref, o_ref, sems):
    pairs = a_ref.shape[0]
    half = a_ref.shape[3]
    hidden = h_ref.shape[1]
    group = 8
    wide = hidden // pieces
    part = half // pieces
    first_loads, last_loads, stores = [], [], []
    for p in range(pieces):
        at = slice(p * wide, (p + 1) * wide)
        first_loads.append(
            [
                pltpu.make_async_copy(g_hbm.at[0, :, at], g_ref.at[p], sems.at[0, p]),
                pltpu.make_async_copy(u_hbm.at[0, :, at], u_ref.at[p], sems.at[1, p]),
            ]
        )
        at = slice(p * part, (p + 1) * part)
        other = slice(half + p * part, half + (p + 1) * part)
        last_loads.append(
            [
                pltpu.make_async_copy(d_hbm.at[0, :, at], d_ref.at[p, 0], sems.at[2, p]),
                pltpu.make_async_copy(d_hbm.at[0, :, other], d_ref.at[p, 1], sems.at[3, p]),
            ]
        )
        stores.append(pltpu.make_async_copy(o_ref.at[p], out_hbm.at[:, :, :, at], sems.at[4, p]))
    loads = first_loads + last_loads
    ahead = 3
    for copies in loads[:ahead]:
        for copy in copies:
            copy.start()
    lower = iota((group, 8, half), 1) < 4
    for i in range(pairs // group):
        tiles = a_ref[i * group : (i + 1) * group].astype(F32)
        first, last = swap_halves(tiles[:, 0], tiles[:, 1], lower)
        at = slice(i * group * 8, (i + 1) * group * 8)
        x_ref[at, 0:half] = first.reshape(group * 8, half).astype(BF16)
        x_ref[at, half:] = last.reshape(group * 8, half).astype(BF16)

    def arrive(n):
        for copy in loads[n]:
            copy.wait()
        if n + ahead < len(loads):
            for copy in loads[n + ahead]:
                copy.start()

    for p in range(pieces):
        arrive(p)
        x = x_ref[...]
        gate = dot(x, g_ref[p])
        up = dot(x, u_ref[p])
        h_ref[:, p * wide : (p + 1) * wide] = (gate * jax.nn.sigmoid(gate) * up).astype(BF16)
    lower = iota((pairs, 8, part), 1) < 4
    for p in range(pieces):
        arrive(pieces + p)
        h = h_ref[...]
        first = dot(h, d_ref[p, 0]).reshape(pairs, 8, part)
        last = dot(h, d_ref[p, 1]).reshape(pairs, 8, part)
        even, odd = swap_halves(first, last, lower)
        o_ref[p, :, 0] = even.astype(BF16)
        o_ref[p, :, 1] = odd.astype(BF16)
        stores[p].start()
    for store in stores:
        store.wait()


def expert_products(arrived, gate_weight, up_weight, down_weight):
    count, rows, half = arrived.shape
    _, width, hidden = gate_weight.shape
    pieces = 4
    shape = (count // 2, 2, rows, half)
    slots = count * rows // 2
    hbm = pl.BlockSpec(memory_space=pltpu.HBM)
    body = lambda *refs: expert_body(pieces, *refs)
    out = pl.pallas_call(
        body,
        in_specs=[pl.BlockSpec(memory_space=pltpu.VMEM), hbm, hbm, hbm],
        out_specs=hbm,
        out_shape=pltpu.HBM(shape, BF16),
        scratch_shapes=[
            pltpu.VMEM((slots, width), BF16),
            pltpu.VMEM((slots, hidden), BF16),
            pltpu.VMEM((pieces, width, hidden // pieces), BF16),
            pltpu.VMEM((pieces, width, hidden // pieces), BF16),
            pltpu.VMEM((pieces, 2, hidden, half // pieces), BF16),
            pltpu.VMEM((pieces, count // 2, 2, rows, half // pieces), BF16),
            pltpu.SemaphoreType.DMA((5, pieces)),
        ],
        compiler_params=params(32),
        cost_estimate=cost(3 * count * rows * width * hidden, 6 * width * hidden),
        name="expert_products",
    )(arrived.reshape(shape), *in_hbm(gate_weight, up_weight, down_weight))
    return out.reshape(arrived.shape)


def shared_body(n_ref, g_ref, u_ref, d_ref, out_ref):
    normed = n_ref[...]
    gate = dot(normed, g_ref[...])
    up = dot(normed, u_ref[...])
    hidden = (gate * jax.nn.sigmoid(gate) * up).astype(BF16)
    out_ref[...] = dot(hidden, d_ref[...])


def shared_expert(normed, gate_weight, up_weight, down_weight):
    tokens, width = normed.shape
    hidden = gate_weight.shape[1]
    return pl.pallas_call(
        shared_body,
        out_shape=pltpu.HBM((tokens, width), F32),
        compiler_params=params(16),
        cost_estimate=cost(6 * tokens * width * hidden, 6 * width * hidden),
        name="shared_expert",
    )(*in_hbm(normed, gate_weight, up_weight, down_weight))


def combine_body(cap, back_ref, rows_ref, weight_ref, shared_hbm, out_hbm, shared_ref, out_ref, sems):
    tokens, _ = out_ref.shape
    total, half = back_ref.shape
    loads, stores = [], []
    for h in range(2):
        cols = slice(h * half, (h + 1) * half)
        loads.append(
            pltpu.make_async_copy(shared_hbm.at[:, cols], shared_ref.at[:, cols], sems.at[0, h])
        )
        stores.append(pltpu.make_async_copy(out_ref.at[:, cols], out_hbm.at[:, cols], sems.at[1, h]))
        loads[h].start()
    row_col = jnp.transpose(rows_ref[...].astype(F32))
    weight_col = jnp.transpose(jnp.concatenate([weight_ref[...]] * 4, axis=0))
    at0, at1 = row_col[:, 0:1].astype(jnp.int32), row_col[:, 1:2].astype(jnp.int32)
    w0, w1 = weight_col[:, 0:1], weight_col[:, 1:2]
    lane = iota((tokens, total), 1)
    for h in range(2):
        cols = slice(h * half, (h + 1) * half)
        mixed = jnp.where(lane == at0 + h * cap, w0, jnp.where(lane == at1 + h * cap, w1, 0.0))
        product = dot(jnp.concatenate(split_two(mixed), axis=0), back_ref[...])
        loads[h].wait()
        routed = product[0:tokens] + product[tokens:]
        out_ref[:, cols] = (routed + shared_ref[:, cols]).astype(BF16)
        stores[h].start()
    for store in stores:
        store.wait()


def combine(back, rows, weights, shared, cap):
    tokens, width = shared.shape
    hbm = pl.BlockSpec(memory_space=pltpu.HBM)
    vmem = pl.BlockSpec(memory_space=pltpu.VMEM)
    body = lambda *refs: combine_body(cap, *refs)
    return pl.pallas_call(
        body,
        in_specs=[vmem, vmem, vmem, hbm],
        out_specs=hbm,
        out_shape=jax.ShapeDtypeStruct((tokens, width), BF16),
        scratch_shapes=[
            pltpu.VMEM((tokens, width), F32),
            pltpu.VMEM((tokens, width), BF16),
            pltpu.SemaphoreType.DMA((2, 2)),
        ],
        compiler_params=params(20),
        cost_estimate=cost(4 * tokens * back.shape[0] * width, 2 * back.size),
        name="combine",
    )(back, rows, weights, *in_hbm(shared))


def gate_rows(in_ref, forget_ref, extra_ref, bias_ref):
    x = forget_ref[...] + bias_ref[0]
    log_forget = jnp.minimum(x, 0.0) - jnp.log1p(jnp.exp(-jnp.abs(x))) + extra_ref[...]
    upper = jnp.where(iota((BLK, BLK), 0) <= iota((BLK, BLK), 1), 1.0, 0.0)
    cumulative = exact_dot(log_forget, upper)
    ones = jnp.ones((BLK, BLK), F32)
    total = exact_dot(log_forget, ones)
    return in_ref[...], cumulative, total


def state_body(k_ref, v_ref, in_ref, forget_ref, extra_ref, bias_ref, out_ref):
    key_dim, length = k_ref.shape
    blocks = length // BLK
    in_gate, cumulative, total = gate_rows(in_ref, forget_ref, extra_ref, bias_ref)
    sums = [jnp.zeros((1, BLK), F32)]
    for j in reversed(range(1, blocks)):
        sums.insert(0, sums[0] + total[j : j + 1, :])
    after = jnp.concatenate(sums, axis=0)
    gap = after + total - cumulative + in_gate
    top = jnp.max(jnp.max(gap, axis=1, keepdims=True), axis=0, keepdims=True)
    weight = jnp.exp(gap - top)
    decay = jnp.sum(total[:, 0:1], axis=0, keepdims=True)
    acc = jnp.zeros((2 * key_dim, 2 * BLK), F32)
    ones = jnp.ones((2 * BLK, BLK), BF16)
    for j in range(blocks // 2):
        at = slice(j * 2 * BLK, (j + 1) * 2 * BLK)
        weights = jnp.concatenate([weight[2 * j : 2 * j + 1], weight[2 * j + 1 : 2 * j + 2]], axis=1)
        keys = k_ref[:, at].astype(F32) * weights
        hi, lo = split_two(keys)
        values = jnp.concatenate([v_ref[at, :], ones], axis=1)
        acc = acc + dot(jnp.concatenate([hi, lo], axis=0), values)
    state = acc[:key_dim] + acc[key_dim:]
    norm = jnp.transpose(state[:, BLK:])[0:8, :]
    norm = jnp.concatenate([norm, jnp.zeros((8, BLK - key_dim), F32)], axis=1)
    lane = iota((8, BLK), 1)
    tail = jnp.where(lane < key_dim, norm, jnp.where(lane < key_dim + 32, top, decay))
    out_ref[0:key_dim, :] = state[:, 0:BLK]
    out_ref[key_dim:, :] = tail


def device_state(keys, values, in_gate, forget, extra, bias):
    key_dim, length = keys.shape
    return pl.pallas_call(
        state_body,
        in_specs=[pl.BlockSpec(memory_space=pltpu.VMEM)] * 5 + [pl.BlockSpec(memory_space=pltpu.SMEM)],
        out_shape=jax.ShapeDtypeStruct((key_dim + 8, BLK), F32),
        compiler_params=params(8),
        cost_estimate=cost(8 * length * key_dim * BLK, 4 * length * BLK),
        name="device_state",
    )(*in_hbm(keys, values, in_gate, forget, extra), bias)


def merge_states(refs, keys, counted, key_dim):
    tails = [ref[key_dim : key_dim + 1, :] for ref in refs]
    tops = [t[:, key_dim : key_dim + 1] for t in tails]
    decays = [
        jnp.where(c, t[:, key_dim + 32 : key_dim + 33], 0.0) for t, c in zip(tails, counted)
    ]
    gaps = []
    for i, key in enumerate(keys):
        since = jnp.zeros((1, 1), F32)
        for j, other in enumerate(keys):
            if j != i:
                since = since + jnp.where(other > key, decays[j], 0.0)
        gaps.append(jnp.where(counted[i], tops[i] + since, NEG))
    top = gaps[0]
    for gap in gaps[1:]:
        top = jnp.maximum(top, gap)
    merged = jnp.zeros((key_dim + 8, BLK), F32)
    for ref, gap, c in zip(refs, gaps, counted):
        merged = merged + ref[...] * jnp.where(c, jnp.exp(gap - top), 0.0)
    return merged, top, sum(decays)


def as_one(scalar):
    return jnp.full((1, 1), scalar, jnp.int32)


def ring_places(place, count):
    return [as_one((place + count - k) % count) for k in range(count)]


def row_body(place_ref, *refs):
    *states, out_ref = refs
    key_dim = out_ref.shape[0] - 8
    keys = ring_places(place_ref[1], len(states))
    counted = [jnp.full((1, 1), True)] * len(states)
    merged, top, decay = merge_states(states, keys, counted, key_dim)
    lane = iota((8, BLK), 1)
    norm = merged[key_dim:, :]
    out_ref[0:key_dim, :] = merged[0:key_dim]
    out_ref[key_dim:, :] = jnp.where(
        lane < key_dim, norm, jnp.where(lane < key_dim + 32, top, decay)
    )


def row_state(place, states):
    return pl.pallas_call(
        row_body,
        in_specs=[pl.BlockSpec(memory_space=pltpu.SMEM)]
        + [pl.BlockSpec(memory_space=pltpu.VMEM)] * len(states),
        out_shape=jax.ShapeDtypeStruct(states[0].shape, F32),
        compiler_params=params(4),
        cost_estimate=cost(2**20, 2**18),
        name="row_state",
    )(place, *states)


def incoming_state(place_ref, rows, columns, key_dim):
    in_row = ring_places(place_ref[1], len(rows))
    in_column = ring_places(place_ref[0], len(columns) + 1)[1:]
    counted = [p < as_one(place_ref[1]) for p in in_row[1:]]
    counted += [p < as_one(place_ref[0]) for p in in_column]
    keys = [p + len(columns) + 1 for p in in_row[1:]] + in_column
    memory, top, _ = merge_states(rows[1:] + columns, keys, counted, key_dim)
    norm = jnp.broadcast_to(memory[key_dim : key_dim + 1, :], (BLK, BLK))
    norm = jnp.transpose(norm)[0:key_dim, :]
    return jnp.concatenate([memory[0:key_dim], norm], axis=1), top


def mixer_body(
    rows_count,
    columns_count,
    place_ref,
    bias_ref,
    q_ref,
    k_ref,
    v_ref,
    in_ref,
    forget_ref,
    extra_ref,
    gate_ref,
    gain_ref,
    *refs,
):
    key_dim, length = k_ref.shape
    blocks = length // BLK
    rows = list(refs[:rows_count])
    columns = list(refs[rows_count : rows_count + columns_count])
    out_ref = refs[-1]
    peers = out_ref.shape[0]
    tokens = length // peers
    per_chunk = tokens // BLK
    in_gate, cumulative, total = gate_rows(in_ref, forget_ref, extra_ref, bias_ref)
    state, top = incoming_state(place_ref, rows, columns, key_dim)
    gap = total - cumulative + in_gate
    block_top = jnp.max(gap, axis=1, keepdims=True)
    weight = jnp.exp(gap - block_top)
    shifted = in_gate - cumulative
    sum_col = jnp.transpose(jnp.concatenate([cumulative] * (BLK // blocks), axis=0))
    ones = jnp.ones((BLK, BLK), BF16)
    lower = iota((BLK, BLK), 1) <= iota((BLK, BLK), 0)
    gain = gain_ref[...]
    eight = jnp.ones((8, BLK), F32)
    squares = []
    for j in range(blocks):
        at = slice(j * BLK, (j + 1) * BLK)
        keys = k_ref[:, at]
        values = jnp.concatenate([v_ref[at, :], ones], axis=1)
        query = jnp.transpose(q_ref[:, at].astype(F32) * (key_dim**-0.5)).astype(BF16)
        base = sum_col[:, j : j + 1]
        pair = jnp.where(lower, base + shifted[j : j + 1, :], -jnp.inf)
        carried = base + top
        stable = jnp.maximum(carried, jnp.max(pair, axis=1, keepdims=True))
        scores = dot(query, keys) * jnp.exp(pair - stable)
        carry = jnp.exp(carried - stable)
        score_hi, score_lo = split_two(scores)
        state_hi, state_lo = split_two(state)
        both = dot(score_hi, values) + dot(score_lo, values)
        both = both + carry * (dot(query, state_hi) + dot(query, state_lo))
        hidden = both[:, :BLK] / jnp.maximum(jnp.abs(both[:, BLK:]), jnp.exp(-stable))
        squares.append(
            exact_dot(eight, hidden * hidden, (((1,), (1,)), ((), ())))[0:1, :]
        )
        gated = hidden * gain * jax.nn.sigmoid(gate_ref[at, :].astype(F32))
        start = (j % per_chunk) * BLK
        out_ref[j // per_chunk, start : start + BLK, :] = gated.astype(BF16)
        if j + 1 < blocks:
            hi, lo = split_two(keys.astype(F32) * weight[j : j + 1, :])
            added = dot(jnp.concatenate([hi, lo], axis=0), values)
            added = added[:key_dim] + added[key_dim:]
            late = block_top[j : j + 1, :]
            early = total[j : j + 1, 0:1] + top
            top = jnp.maximum(early, late)
            state = jnp.exp(early - top) * state + jnp.exp(late - top) * added
    for c in range(peers):
        own = squares[c * per_chunk : (c + 1) * per_chunk]
        parts = [split_two(row) for row in own]
        rows = [hi.astype(F32) for hi, _ in parts] + [lo.astype(F32) for _, lo in parts]
        rows.append(jnp.zeros((16 - len(rows), BLK), F32))
        out_ref[c, tokens:, :] = jnp.concatenate(rows, axis=0).astype(BF16)


def mixer_rows(place, bias, rows, columns, queries, keys, values, in_gate, forget, extra, gate, gain, peers):
    _, length = keys.shape
    smem = pl.BlockSpec(memory_space=pltpu.SMEM)
    vmem = pl.BlockSpec(memory_space=pltpu.VMEM)
    chunk = (length // peers + 16, BLK)
    body = lambda *refs: mixer_body(len(rows), len(columns), *refs)
    return pl.pallas_call(
        body,
        in_specs=[smem, smem] + [vmem] * (8 + len(rows) + len(columns)),
        out_shape=pltpu.HBM((peers, *chunk), BF16),
        compiler_params=params(16),
        cost_estimate=cost(32 * length * BLK * BLK, 8 * length * BLK),
        name="mixer_rows",
    )(
        place,
        bias,
        *in_hbm(queries, keys, values, in_gate, forget, extra, gate, gain),
        *rows,
        *columns,
    )


def project_body(g_ref, w_ref, out_ref, scale_ref):
    heads = g_ref.shape[0]
    tokens = out_ref.shape[0]
    per_chunk = tokens // BLK

    @pl.when(pl.program_id(0) == 0)
    def _():
        tail = g_ref[0, tokens:, :].astype(F32)
        for h in range(1, heads):
            tail = tail + g_ref[h, tokens:, :].astype(F32)
        for c in range(per_chunk):
            row = tail[c : c + 1, :] + tail[per_chunk + c : per_chunk + c + 1, :]
            row = lax.rsqrt(row / (heads * BLK) + 1e-06)
            scale_ref[c * BLK : (c + 1) * BLK, :] = jnp.transpose(jnp.broadcast_to(row, (BLK, BLK)))

    mixed = jnp.concatenate([g_ref[h, 0:tokens, :] for h in range(heads)], axis=1)
    product = dot(mixed, w_ref[...])
    out_ref[...] = (product * scale_ref[:, 0:1]).astype(BF16)


def project(gathered, weight):
    _, rows, _ = gathered.shape
    tokens = rows - 16
    width = weight.shape[1]
    steps = 4
    return pl.pallas_call(
        project_body,
        grid=(steps,),
        in_specs=[
            whole(gathered.shape),
            pl.BlockSpec((weight.shape[0], width // steps), lambda i: (0, i)),
        ],
        out_specs=pl.BlockSpec((tokens, width // steps), lambda i: (0, i)),
        out_shape=jax.ShapeDtypeStruct((tokens, width), BF16),
        scratch_shapes=[pltpu.VMEM((tokens, BLK), F32)],
        compiler_params=params(16, True),
        cost_estimate=cost(2 * tokens * weight.size, 2 * weight.size),
        name="project",
    )(gathered, *in_hbm(weight))


def exchange(x, axes):
    return lax.all_to_all(x, axes, split_axis=0, concat_axis=0, tiled=True)


def from_earlier(x, axis):
    count = lax.axis_size(axis)
    return [
        lax.ppermute(x, axis, [(p, (p + k) % count) for p in range(count)])
        for k in range(1, count)
    ]


def on_one(
    queries,
    head_key_rows,
    head_value_rows,
    log_input_gate,
    forget_logits,
    head_forget_bias,
    extra_log_forget,
    output_gate_logits,
    head_norm_gain,
    mixer_output_weight,
    second_batch_input,
    expert_norm_gain,
    routed_expert_index,
    routed_copy_weight,
    routed_gate_weight,
    routed_up_weight,
    routed_down_weight,
    shared_gate_weight,
    shared_up_weight,
    shared_down_weight,
):
    length = queries.shape[0]
    ep_count, tp_count = lax.axis_size(EP), lax.axis_size("tp")
    experts = ep_count * tp_count
    cap = 4
    send, normed, rows = dispatch_rows(
        second_batch_input, expert_norm_gain[None, :], routed_expert_index.T, cap, experts
    )
    landed = exchange(send.reshape(experts, 2 * cap, -1), EP_TP)

    def by_block(a):
        return a.reshape(length // BLK, BLK)

    in_gate, forget, extra = (
        by_block(log_input_gate),
        by_block(forget_logits),
        by_block(extra_log_forget),
    )
    query_rows, key_rows = queries.T, head_key_rows.T
    place = jnp.stack([lax.axis_index(a).astype(jnp.int32) for a in ("ep_0", "ep_1", "tp")])
    own = device_state(key_rows, head_value_rows, in_gate, forget, extra, head_forget_bias)
    row_states = [own] + from_earlier(own, "ep_1")
    row_total = row_state(place, row_states)
    column_states = from_earlier(row_total, "ep_0")
    mixed = mixer_rows(
        place,
        head_forget_bias,
        row_states,
        column_states,
        query_rows,
        key_rows,
        head_value_rows,
        in_gate,
        forget,
        extra,
        output_gate_logits,
        head_norm_gain[None, :],
        tp_count,
    )
    shared = shared_expert(normed, shared_gate_weight, shared_up_weight, shared_down_weight)
    gathered = exchange(mixed, "tp")
    produced = expert_products(landed, routed_gate_weight, routed_up_weight, routed_down_weight)
    back = exchange(produced, EP_TP)
    mixer_first_output = project(gathered, mixer_output_weight)
    moe_out = combine(
        back.reshape(experts * 2 * cap, -1), rows, routed_copy_weight.T, shared, cap
    )
    return (mixer_first_output, moe_out)


def solution(mesh):
    split = Mesh(mesh.devices.reshape(4, 4, mesh.shape["tp"]), ("ep_0", "ep_1", "tp"))
    return jax.shard_map(
        on_one,
        mesh=split,
        in_specs=(
            P(EP, "tp"),
            P(EP, "tp"),
            P(EP, "tp"),
            P(EP, "tp"),
            P(EP, "tp"),
            P("tp"),
            P(EP, "tp"),
            P(EP, "tp"),
            P("tp"),
            P(),
            P(EP_TP, None),
            P(),
            P(EP_TP, None),
            P(EP_TP, None),
            P(EP_TP, None, None),
            P(EP_TP, None, None),
            P(EP_TP, None, None),
            P(),
            P(),
            P(),
        ),
        out_specs=(P(EP_TP, None), P(EP_TP, None)),
        check_vma=False,
    )
```

profile of v0, /device:TPU:1, one launch (start us, length us, event | category | flops | bytes accessed | tf_op | source)
XLA Modules:
  0.0 117.5 jit_solution(5625907349912086660)
XLA Ops:
  0.6 4.5 %dispatch_rows.1 = (bf16[1024,1024]{1,0:T(8,128)(2,1)}, bf16[192,2048]{1,0:T(8,128)(2,1)}, s32[8,192]{1,0:T(8,128)}) custom-call(bf16[192,2048]{1,0:T(8,128)(2,1)} %refs_0_.1, f32[1,2048]{1,0:T(1,128)} %bitcast.30, s32[2,192]{1,0:T(2,128)} %bitcast.31), custom_call_target="tpu_custom_call" | custom-call | flops 805306368 | bytes 8388608 | tf_op jit(solution)/shard_map/dispatch_rows/pallas_call | solution.py:102
  5.2 11.5 %all-to-all-start.1 = ((bf16[128,8,1024]{2,1,0:T(8,128)(2,1)}), bf16[128,8,1024]{2,1,0:T(8,128)(2,1)S(1)}, u32[]{:S(2)}, u32[]{:S(2)}) async-start(bf16[128,8,1024]{2,1,0:T(8,128)(2,1)} %bitcast.19), calls=%async_computation.1 | async-start | bytes 4194304 | tf_op jit(solution)/shard_map/all_to_all | solution.py:549
  17.3 1.8 %device_state.1.refs_0_.refs_10_ = f32[72,128]{1,0:T(8,128)S(1)} custom-call(bf16[64,2048]{1,0:T(8,128)(2,1)} %bitcast.21, bf16[2048,128]{1,0:T(8,128)(2,1)} %refs_4_.1, f32[16,128]{1,0:T(8,128)} %bitcast.23, f32[16,128]{1,0:T(8,128)} %bitcast.25, f32[16,128]{1,0:T(8,128)} %bitcast.27, f32[1]{0:T(128)S(6)} %copy.22.bias_ref.refs_1_), custom_call_target="tpu_custom_call" | custom-call | flops 134217728 | bytes 1048576 | tf_op jit(solution)/shard_map/device_state/pallas_call | solution.py:334
  19.2 2.6 %collective-permute-start.2 = (f32[72,128]{1,0:T(8,128)S(1)}, f32[72,128]{1,0:T(8,128)S(1)}, u32[]{:S(2)}, u32[]{:S(2)}) collective-permute-start(f32[72,128]{1,0:T(8,128)S(1)} %device_state.1.refs_0_.refs_10_), channel_id=1, source_target_pairs={{0,24},{8,0},{16,8},{24,16},{1,25},{9,1},{17,9},{25,17},{2,26},{10... | collective-permute-start | bytes 110600 | tf_op jit(solution)/shard_map/ppermute | solution.py:555
  21.8 0.6 collective-permute-start.1
  22.3 0.6 collective-permute-start
  22.9 0.1 pad_add_fusion.place_ref.refs_0_
  23.0 18.3 %collective-permute-done.2.refs_3_.refs_13_ = f32[72,128]{1,0:T(8,128)S(1)} collective-permute-done((f32[72,128]{1,0:T(8,128)S(1)}, f32[72,128]{1,0:T(8,128)S(1)}, u32[]{:S(2)}, u32[]{:S(2)}) %collective-permute-start.2) | collective-permute-done | bytes 36896 | tf_op jit(solution)/shard_map/ppermute | solution.py:555
  41.3 1.5 %collective-permute-done.1.refs_2_.refs_12_ = f32[72,128]{1,0:T(8,128)S(1)} collective-permute-done((f32[72,128]{1,0:T(8,128)S(1)}, f32[72,128]{1,0:T(8,128)S(1)}, u32[]{:S(2)}, u32[]{:S(2)}) %collective-permute-start.1) | collective-permute-done | bytes 36896 | tf_op jit(solution)/shard_map/ppermute | solution.py:555
  42.8 0.3 collective-permute-done.refs_1_.refs_11_
  43.1 0.8 row_state.1
  43.8 3.2 %collective-permute-start.5 = (f32[72,128]{1,0:T(8,128)S(1)}, f32[72,128]{1,0:T(8,128)S(1)}, u32[]{:S(2)}, u32[]{:S(2)}) collective-permute-start(f32[72,128]{1,0:T(8,128)S(1)} %row_state.1), channel_id=1, source_target_pairs={{0,96},{32,0},{64,32},{96,64},{1,97},{33,1},{65,33},{97,65},{2,98}... | collective-permute-start | bytes 110600 | tf_op jit(solution)/shard_map/ppermute | solution.py:555
  47.0 0.1 collective-permute-start.4
  47.1 0.8 collective-permute-start.3
  47.9 0.2 collective-permute-done.5.refs_16_
  48.1 3.3 %collective-permute-done.4.refs_15_ = f32[72,128]{1,0:T(8,128)S(1)} collective-permute-done((f32[72,128]{1,0:T(8,128)S(1)}, f32[72,128]{1,0:T(8,128)S(1)}, u32[]{:S(2)}, u32[]{:S(2)}) %collective-permute-start.4) | collective-permute-done | bytes 36896 | tf_op jit(solution)/shard_map/ppermute | solution.py:555
  51.4 0.1 collective-permute-done.3.refs_14_
  51.5 8.3 %mixer_rows.1 = bf16[8,272,128]{2,1,0:T(8,128)(2,1)} custom-call(s32[3]{0:T(128)S(1)} %pad_add_fusion.place_ref.refs_0_, f32[1]{0:T(128)S(6)} %copy.22.bias_ref.refs_1_, bf16[64,2048]{1,0:T(8,128)(2,1)} %bitcast.29, bf16[64,2048]{1,0:T(8,128)(2,1)} %bitcast.22, bf16[2048,128]{1,0:T(8,128)(2,1)} %refs_4_.1, f32[16,128]{1,0:T(8,128)} %bitcast.24, ...), custom_call_target="tpu_custom_call" | custom-call | flops 1073741824 | bytes 2097152 | tf_op jit(solution)/shard_map/mixer_rows/pallas_call | solution.py:491
  59.9 0.0 all-to-all-done.1
  59.9 7.2 %all-to-all-start = ((bf16[8,272,128]{2,1,0:T(8,128)(2,1)}), bf16[8,272,128]{2,1,0:T(8,128)(2,1)S(1)}, u32[]{:S(2)}, u32[]{:S(2)}) async-start(bf16[8,272,128]{2,1,0:T(8,128)(2,1)} %mixer_rows.1), calls=%async_computation | async-start | bytes 1114112 | tf_op jit(solution)/shard_map/all_to_all | solution.py:549
  67.1 10.5 %expert_products.1 = bf16[64,2,8,1024]{3,2,1,0:T(8,128)(2,1)} custom-call(bf16[64,2,8,1024]{3,2,1,0:T(8,128)(2,1)S(1)} %bitcast.16, bf16[1,2048,1024]{2,1,0:T(8,128)(2,1)} %refs_1_.2, bf16[1,2048,1024]{2,1,0:T(8,128)(2,1)} %refs_2_.1, bf16[1,1024,2048]{2,1,0:T(8,128)(2,1)} %refs_3_.1), custom_call_target="tpu_custom_call" | custom-call | flops 6442450944 | bytes 12582912 | tf_op jit(solution)/shard_map/expert_products/pallas_call | solution.py:202
  77.5 0.0 all-to-all-done.g_ref
  77.5 6.3 %all-to-all-start.2 = ((bf16[128,8,1024]{2,1,0:T(8,128)(2,1)}), bf16[128,8,1024]{2,1,0:T(8,128)(2,1)S(1)}, u32[]{:S(2)}, u32[]{:S(2)}) async-start(bf16[128,8,1024]{2,1,0:T(8,128)(2,1)} %bitcast.20), calls=%async_computation.2 | async-start | bytes 4194304 | tf_op jit(solution)/shard_map/all_to_all | solution.py:549
  83.9 5.2 %shared_expert.1.refs_3_ = f32[192,2048]{1,0:T(8,128)} custom-call(bf16[192,2048]{1,0:T(8,128)(2,1)} %get-tuple-element.7.n_ref, bf16[2048,384]{1,0:T(8,128)(2,1)} %g_ref.1, bf16[2048,384]{1,0:T(8,128)(2,1)} %u_ref.1, bf16[384,2048]{1,0:T(8,128)(2,1)} %d_ref.1), custom_call_target="tpu_custom_call" | custom-call | flops 905969664 | bytes 4718592 | tf_op jit(solution)/shard_map/shared_expert/pallas_call | solution.py:234
  89.1 0.0 copy-start
  89.1 0.0 copy-start.1
  89.1 5.0 %project.1 = bf16[256,2048]{1,0:T(8,128)(2,1)} custom-call(bf16[8,272,128]{2,1,0:T(8,128)(2,1)S(1)} %all-to-all-done.g_ref, bf16[1024,2048]{1,0:T(8,128)(2,1)} %w_ref.1), custom_call_target="tpu_custom_call" | custom-call | flops 1073741824 | bytes 4194304 | tf_op jit(solution)/shard_map/project/pallas_call | solution.py:532
  94.1 19.9 %all-to-all-done.2 = bf16[128,8,1024]{2,1,0:T(8,128)(2,1)S(1)} async-done(((bf16[128,8,1024]{2,1,0:T(8,128)(2,1)}), bf16[128,8,1024]{2,1,0:T(8,128)(2,1)S(1)}, u32[]{:S(2)}, u32[]{:S(2)}) %all-to-all-start.2) | async-done | bytes 2097184 | tf_op jit(solution)/shard_map/all_to_all | solution.py:549
  114.0 0.0 copy-done
  114.0 0.0 copy-done.1
  114.0 3.3 %combine.1 = bf16[192,2048]{1,0:T(8,128)(2,1)} custom-call(bf16[1024,1024]{1,0:T(8,128)(2,1)S(1)} %bitcast.17, s32[8,192]{1,0:T(8,128)S(1)} %copy-done.1, f32[2,192]{1,0:T(2,128)S(1)} %bitcast.18, f32[192,2048]{1,0:T(8,128)} %shared_expert.1.refs_3_), custom_call_target="tpu_custom_call" | custom-call | flops 1610612736 | bytes 2097152 | tf_op jit(solution)/shard_map/combine/pallas_call | solution.py:276
Async XLA Ops:
  5.2 54.7 %all-to-all-start.1 = ((bf16[128,8,1024]{2,1,0:T(8,128)(2,1)}), bf16[128,8,1024]{2,1,0:T(8,128)(2,1)S(1)}, u32[]{:S(2)}, u32[]{:S(2)}) async-start(bf16[128,8,1024]{2,1,0:T(8,128)(2,1)} %bitcast.19), calls=%async_computation.1 | async-start | bytes 4194304 | tf_op jit(solution)/shard_map/all_to_all | solution.py:549
  19.2 22.1 %collective-permute-start.2 = (f32[72,128]{1,0:T(8,128)S(1)}, f32[72,128]{1,0:T(8,128)S(1)}, u32[]{:S(2)}, u32[]{:S(2)}) collective-permute-start(f32[72,128]{1,0:T(8,128)S(1)} %device_state.1.refs_0_.refs_10_), channel_id=1, source_target_pairs={{0,24},{8,0},{16,8},{24,16},{1,25},{9,1},{17,9},{25,17},{2,26},{10... | collective-permute-start | bytes 110600 | tf_op jit(solution)/shard_map/ppermute | solution.py:555
  21.8 21.0 %collective-permute-start.1 = (f32[72,128]{1,0:T(8,128)S(1)}, f32[72,128]{1,0:T(8,128)S(1)}, u32[]{:S(2)}, u32[]{:S(2)}) collective-permute-start(f32[72,128]{1,0:T(8,128)S(1)} %device_state.1.refs_0_.refs_10_), channel_id=1, source_target_pairs={{0,16},{8,24},{16,0},{24,8},{1,17},{9,25},{17,1},{25,9},{2,18},{10... | collective-permute-start | bytes 110600 | tf_op jit(solution)/shard_map/ppermute | solution.py:555
  22.3 20.7 %collective-permute-start = (f32[72,128]{1,0:T(8,128)S(1)}, f32[72,128]{1,0:T(8,128)S(1)}, u32[]{:S(2)}, u32[]{:S(2)}) collective-permute-start(f32[72,128]{1,0:T(8,128)S(1)} %device_state.1.refs_0_.refs_10_), channel_id=1, source_target_pairs={{0,8},{8,16},{16,24},{24,0},{1,9},{9,17},{17,25},{25,1},{2,10},{10... | collective-permute-start | bytes 110600 | tf_op jit(solution)/shard_map/ppermute | solution.py:555
  43.8 4.2 %collective-permute-start.5 = (f32[72,128]{1,0:T(8,128)S(1)}, f32[72,128]{1,0:T(8,128)S(1)}, u32[]{:S(2)}, u32[]{:S(2)}) collective-permute-start(f32[72,128]{1,0:T(8,128)S(1)} %row_state.1), channel_id=1, source_target_pairs={{0,96},{32,0},{64,32},{96,64},{1,97},{33,1},{65,33},{97,65},{2,98}... | collective-permute-start | bytes 110600 | tf_op jit(solution)/shard_map/ppermute | solution.py:555
  47.0 4.4 %collective-permute-start.4 = (f32[72,128]{1,0:T(8,128)S(1)}, f32[72,128]{1,0:T(8,128)S(1)}, u32[]{:S(2)}, u32[]{:S(2)}) collective-permute-start(f32[72,128]{1,0:T(8,128)S(1)} %row_state.1), channel_id=1, source_target_pairs={{0,64},{32,96},{64,0},{96,32},{1,65},{33,97},{65,1},{97,33},{2,66}... | collective-permute-start | bytes 110600 | tf_op jit(solution)/shard_map/ppermute | solution.py:555
  47.1 4.4 %collective-permute-start.3 = (f32[72,128]{1,0:T(8,128)S(1)}, f32[72,128]{1,0:T(8,128)S(1)}, u32[]{:S(2)}, u32[]{:S(2)}) collective-permute-start(f32[72,128]{1,0:T(8,128)S(1)} %row_state.1), channel_id=1, source_target_pairs={{0,32},{32,64},{64,96},{96,0},{1,33},{33,65},{65,97},{97,1},{2,34}... | collective-permute-start | bytes 110600 | tf_op jit(solution)/shard_map/ppermute | solution.py:555
  59.9 17.6 %all-to-all-start = ((bf16[8,272,128]{2,1,0:T(8,128)(2,1)}), bf16[8,272,128]{2,1,0:T(8,128)(2,1)S(1)}, u32[]{:S(2)}, u32[]{:S(2)}) async-start(bf16[8,272,128]{2,1,0:T(8,128)(2,1)} %mixer_rows.1), calls=%async_computation | async-start | bytes 1114112 | tf_op jit(solution)/shard_map/all_to_all | solution.py:549
  77.5 36.4 %all-to-all-start.2 = ((bf16[128,8,1024]{2,1,0:T(8,128)(2,1)}), bf16[128,8,1024]{2,1,0:T(8,128)(2,1)S(1)}, u32[]{:S(2)}, u32[]{:S(2)}) async-start(bf16[128,8,1024]{2,1,0:T(8,128)(2,1)} %bitcast.20), calls=%async_computation.2 | async-start | bytes 4194304 | tf_op jit(solution)/shard_map/all_to_all | solution.py:549
  89.1 24.9 %copy-start = (f32[192,2]{0,1:T(2,128)S(1)}, f32[192,2]{0,1:T(2,128)}, u32[]{:S(2)}) copy-start(f32[192,2]{0,1:T(2,128)} %param.33) | copy-start | bytes 4612
  89.1 24.9 %copy-start.1 = (s32[8,192]{1,0:T(8,128)S(1)}, s32[8,192]{1,0:T(8,128)}, u32[]{:S(2)}) copy-start(s32[8,192]{1,0:T(8,128)} %get-tuple-element.6.refs_1_) | copy-start | bytes 18436
where the time goes:
time: 118 us; the launch traced here: 117 us
  waiting for transfers between devices  43.6 us (37%)
  Pallas kernels  39.4 us (33%)
  starting transfers between devices  32.8 us (28%)
  between operations  1.49 us (1%)
    all_to_all x3, starting transfers between devices, exchange(): return lax.all_to_all(x, axes, split_axis=0, concat_axis=0, tiled=True)  25 us
    ppermute x6, waiting for transfers between devices, from_earlier(): lax.ppermute(x, axis, [(p, (p + k) % count) for p in range(count)])  23.7 us
    all_to_all x3, waiting for transfers between devices, exchange(): return lax.all_to_all(x, axes, split_axis=0, concat_axis=0, tiled=True)  19.9 us
    pallas_call x1, Pallas kernels, expert_products(): pl.pallas_call(body, in_specs=[pl.BlockSpec(memory_space=pltpu.VMEM), hbm...  10.5 us
    pallas_call x1, Pallas kernels, mixer_rows(): pl.pallas_call(body, in_specs=[smem, smem] + [vmem] * (8 + len(rows) + le...  8.34 us
    ppermute x6, starting transfers between devices, from_earlier(): lax.ppermute(x, axis, [(p, (p + k) % count) for p in range(count)])  7.81 us
    pallas_call x1, Pallas kernels, shared_expert(): pl.pallas_call(shared_body, out_shape=pltpu.HBM((tokens, width), F32), co...  5.25 us
    pallas_call x1, Pallas kernels, project(): pl.pallas_call(project_body, grid=(steps,), in_specs=[whole(gathered.shap...  4.95 us
  transfers between devices with their start and end apart: 9, of which 7 were waited for; matrix products, arithmetic and copies ran while one was open for 0% of the time, Pallas kernels for 27%

commit v1 on v0

--- a/solution.py
+++ b/solution.py
@@ -341,77 +341,26 @@
     )(*in_hbm(keys, values, in_gate, forget, extra), bias)
 
 
-def merge_states(refs, keys, counted, key_dim):
-    tails = [ref[key_dim : key_dim + 1, :] for ref in refs]
-    tops = [t[:, key_dim : key_dim + 1] for t in tails]
-    decays = [
-        jnp.where(c, t[:, key_dim + 32 : key_dim + 33], 0.0) for t, c in zip(tails, counted)
-    ]
-    gaps = []
-    for i, key in enumerate(keys):
-        since = jnp.zeros((1, 1), F32)
-        for j, other in enumerate(keys):
-            if j != i:
-                since = since + jnp.where(other > key, decays[j], 0.0)
-        gaps.append(jnp.where(counted[i], tops[i] + since, NEG))
-    top = gaps[0]
-    for gap in gaps[1:]:
-        top = jnp.maximum(top, gap)
-    merged = jnp.zeros((key_dim + 8, BLK), F32)
-    for ref, gap, c in zip(refs, gaps, counted):
-        merged = merged + ref[...] * jnp.where(c, jnp.exp(gap - top), 0.0)
-    return merged, top, sum(decays)
-
-
-def as_one(scalar):
-    return jnp.full((1, 1), scalar, jnp.int32)
-
-
-def ring_places(place, count):
-    return [as_one((place + count - k) % count) for k in range(count)]
-
-
-def row_body(place_ref, *refs):
-    *states, out_ref = refs
-    key_dim = out_ref.shape[0] - 8
-    keys = ring_places(place_ref[1], len(states))
-    counted = [jnp.full((1, 1), True)] * len(states)
-    merged, top, decay = merge_states(states, keys, counted, key_dim)
-    lane = iota((8, BLK), 1)
-    norm = merged[key_dim:, :]
-    out_ref[0:key_dim, :] = merged[0:key_dim]
-    out_ref[key_dim:, :] = jnp.where(
-        lane < key_dim, norm, jnp.where(lane < key_dim + 32, top, decay)
-    )
-
-
-def row_state(place, states):
-    return pl.pallas_call(
-        row_body,
-        in_specs=[pl.BlockSpec(memory_space=pltpu.SMEM)]
-        + [pl.BlockSpec(memory_space=pltpu.VMEM)] * len(states),
-        out_shape=jax.ShapeDtypeStruct(states[0].shape, F32),
-        compiler_params=params(4),
-        cost_estimate=cost(2**20, 2**18),
-        name="row_state",
-    )(place, *states)
-
-
-def incoming_state(place_ref, rows, columns, key_dim):
-    in_row = ring_places(place_ref[1], len(rows))
-    in_column = ring_places(place_ref[0], len(columns) + 1)[1:]
-    counted = [p < as_one(place_ref[1]) for p in in_row[1:]]
-    counted += [p < as_one(place_ref[0]) for p in in_column]
-    keys = [p + len(columns) + 1 for p in in_row[1:]] + in_column
-    memory, top, _ = merge_states(rows[1:] + columns, keys, counted, key_dim)
+def incoming_state(place, states, key_dim):
+    since = jnp.zeros((1, 1), F32)
+    gaps, counted = [], []
+    top = jnp.full((1, 1), NEG, F32)
+    for k, ref in enumerate(states, 1):
+        tail = ref[key_dim : key_dim + 1, :]
+        counted.append(jnp.full((1, 1), k, jnp.int32) <= place)
+        gaps.append(jnp.where(counted[-1], tail[:, key_dim : key_dim + 1] + since, NEG))
+        since = since + tail[:, key_dim + 32 : key_dim + 33]
+        top = jnp.maximum(top, gaps[-1])
+    memory = jnp.zeros((key_dim + 8, BLK), F32)
+    for ref, gap, c in zip(states, gaps, counted):
+        memory = memory + ref[...] * jnp.where(c, jnp.exp(gap - top), 0.0)
     norm = jnp.broadcast_to(memory[key_dim : key_dim + 1, :], (BLK, BLK))
     norm = jnp.transpose(norm)[0:key_dim, :]
     return jnp.concatenate([memory[0:key_dim], norm], axis=1), top
 
 
 def mixer_body(
-    rows_count,
-    columns_count,
+    state_count,
     place_ref,
     bias_ref,
     q_ref,
@@ -426,14 +375,13 @@
 ):
     key_dim, length = k_ref.shape
     blocks = length // BLK
-    rows = list(refs[:rows_count])
-    columns = list(refs[rows_count : rows_count + columns_count])
-    out_ref = refs[-1]
-    peers = out_ref.shape[0]
+    states = refs[:state_count]
+    *outs, out_ref = refs[state_count:]
+    peers = len(outs)
     tokens = length // peers
     per_chunk = tokens // BLK
     in_gate, cumulative, total = gate_rows(in_ref, forget_ref, extra_ref, bias_ref)
-    state, top = incoming_state(place_ref, rows, columns, key_dim)
+    state, top = incoming_state(place_ref[0], states, key_dim)
     gap = total - cumulative + in_gate
     block_top = jnp.max(gap, axis=1, keepdims=True)
     weight = jnp.exp(gap - block_top)
@@ -480,18 +428,21 @@
         rows = [hi.astype(F32) for hi, _ in parts] + [lo.astype(F32) for _, lo in parts]
         rows.append(jnp.zeros((16 - len(rows), BLK), F32))
         out_ref[c, tokens:, :] = jnp.concatenate(rows, axis=0).astype(BF16)
-
-
-def mixer_rows(place, bias, rows, columns, queries, keys, values, in_gate, forget, extra, gate, gain, peers):
+    for k in range(peers):
+        outs[k][...] = out_ref[(place_ref[1] + k) % peers]
+
+
+def mixer_rows(place, bias, states, queries, keys, values, in_gate, forget, extra, gate, gain, peers):
     _, length = keys.shape
     smem = pl.BlockSpec(memory_space=pltpu.SMEM)
     vmem = pl.BlockSpec(memory_space=pltpu.VMEM)
     chunk = (length // peers + 16, BLK)
-    body = lambda *refs: mixer_body(len(rows), len(columns), *refs)
+    body = lambda *refs: mixer_body(len(states), *refs)
     return pl.pallas_call(
         body,
-        in_specs=[smem, smem] + [vmem] * (8 + len(rows) + len(columns)),
-        out_shape=pltpu.HBM((peers, *chunk), BF16),
+        in_specs=[smem, smem] + [vmem] * (8 + len(states)),
+        out_shape=[jax.ShapeDtypeStruct(chunk, BF16)] * peers,
+        scratch_shapes=[pltpu.VMEM((peers, *chunk), BF16)],
         compiler_params=params(16),
         cost_estimate=cost(32 * length * BLK * BLK, 8 * length * BLK),
         name="mixer_rows",
@@ -499,61 +450,66 @@
         place,
         bias,
         *in_hbm(queries, keys, values, in_gate, forget, extra, gate, gain),
-        *rows,
-        *columns,
-    )
-
-
-def project_body(g_ref, w_ref, out_ref, scale_ref):
-    heads = g_ref.shape[0]
+        *states,
+    )
+
+
+def project_body(heads, place_ref, *refs):
+    chunks = refs[:heads]
+    w_ref, out_ref, all_ref, scale_ref = refs[heads:]
     tokens = out_ref.shape[0]
     per_chunk = tokens // BLK
 
     @pl.when(pl.program_id(0) == 0)
     def _():
-        tail = g_ref[0, tokens:, :].astype(F32)
-        for h in range(1, heads):
-            tail = tail + g_ref[h, tokens:, :].astype(F32)
+        tail = chunks[0][tokens:, :].astype(F32)
+        for k in range(1, heads):
+            tail = tail + chunks[k][tokens:, :].astype(F32)
         for c in range(per_chunk):
             row = tail[c : c + 1, :] + tail[per_chunk + c : per_chunk + c + 1, :]
             row = lax.rsqrt(row / (heads * BLK) + 1e-06)
             scale_ref[c * BLK : (c + 1) * BLK, :] = jnp.transpose(jnp.broadcast_to(row, (BLK, BLK)))
-
-    mixed = jnp.concatenate([g_ref[h, 0:tokens, :] for h in range(heads)], axis=1)
+        for k in range(heads):
+            all_ref[(place_ref[1] + heads - k) % heads] = chunks[k][0:tokens, :]
+
+    mixed = jnp.concatenate([all_ref[h] for h in range(heads)], axis=1)
     product = dot(mixed, w_ref[...])
     out_ref[...] = (product * scale_ref[:, 0:1]).astype(BF16)
 
 
-def project(gathered, weight):
-    _, rows, _ = gathered.shape
+def project(place, chunks, weight):
+    heads = len(chunks)
+    rows = chunks[0].shape[0]
     tokens = rows - 16
     width = weight.shape[1]
     steps = 4
+    body = lambda *refs: project_body(heads, *refs)
     return pl.pallas_call(
-        project_body,
+        body,
         grid=(steps,),
-        in_specs=[
-            whole(gathered.shape),
-            pl.BlockSpec((weight.shape[0], width // steps), lambda i: (0, i)),
-        ],
+        in_specs=[pl.BlockSpec(memory_space=pltpu.SMEM)]
+        + [whole((rows, BLK))] * heads
+        + [pl.BlockSpec((weight.shape[0], width // steps), lambda i: (0, i))],
         out_specs=pl.BlockSpec((tokens, width // steps), lambda i: (0, i)),
         out_shape=jax.ShapeDtypeStruct((tokens, width), BF16),
-        scratch_shapes=[pltpu.VMEM((tokens, BLK), F32)],
+        scratch_shapes=[pltpu.VMEM((heads, tokens, BLK), BF16), pltpu.VMEM((tokens, BLK), F32)],
         compiler_params=params(16, True),
         cost_estimate=cost(2 * tokens * weight.size, 2 * weight.size),
         name="project",
-    )(gathered, *in_hbm(weight))
+    )(place, *chunks, *in_hbm(weight))
 
 
 def exchange(x, axes):
     return lax.all_to_all(x, axes, split_axis=0, concat_axis=0, tiled=True)
 
 
-def from_earlier(x, axis):
-    count = lax.axis_size(axis)
+def from_earlier(shards, axes, wrap):
+    count = lax.axis_size(axes)
     return [
-        lax.ppermute(x, axis, [(p, (p + k) % count) for p in range(count)])
-        for k in range(1, count)
+        lax.ppermute(
+            shard, axes, [(p, (p + k) % count) for p in range(count if wrap else count - k)]
+        )
+        for k, shard in enumerate(shards, 1)
     ]
 
 
@@ -597,16 +553,13 @@
         by_block(extra_log_forget),
     )
     query_rows, key_rows = queries.T, head_key_rows.T
-    place = jnp.stack([lax.axis_index(a).astype(jnp.int32) for a in ("ep_0", "ep_1", "tp")])
+    place = jnp.stack([lax.axis_index(a).astype(jnp.int32) for a in (EP, "tp")])
     own = device_state(key_rows, head_value_rows, in_gate, forget, extra, head_forget_bias)
-    row_states = [own] + from_earlier(own, "ep_1")
-    row_total = row_state(place, row_states)
-    column_states = from_earlier(row_total, "ep_0")
-    mixed = mixer_rows(
+    states = from_earlier([own] * (ep_count - 1), EP, False)
+    chunks = mixer_rows(
         place,
         head_forget_bias,
-        row_states,
-        column_states,
+        states,
         query_rows,
         key_rows,
         head_value_rows,
@@ -618,10 +571,10 @@
         tp_count,
     )
     shared = shared_expert(normed, shared_gate_weight, shared_up_weight, shared_down_weight)
-    gathered = exchange(mixed, "tp")
+    gathered = [chunks[0]] + from_earlier(chunks[1:], "tp", True)
     produced = expert_products(landed, routed_gate_weight, routed_up_weight, routed_down_weight)
     back = exchange(produced, EP_TP)
-    mixer_first_output = project(gathered, mixer_output_weight)
+    mixer_first_output = project(place, gathered, mixer_output_weight)
     moe_out = combine(
         back.reshape(experts * 2 * cap, -1), rows, routed_copy_weight.T, shared, cap
     )

time: 118 us -> 151 us (1.28)
  blocking collectives: 0 us -> 41.6 us
  waiting for transfers between devices: 43.6 us -> 6.24 us
  starting transfers between devices: 32.8 us -> 61.6 us
    ppermute x6 -> x22, starting transfers between devices: 7.81 us -> 56.8 us  [from_earlier(): lax.ppermute(shard, axes, [(p, (p + k) % count) for p in range(count if w...]
    all_to_all x0 -> x1, blocking collectives: none -> 41.6 us  [exchange(): return lax.all_to_all(x, axes, split_axis=0, concat_axis=0, tiled=True)]
    all_to_all x3 -> x1, starting transfers between devices: 25 us -> 4.76 us  [exchange(): return lax.all_to_all(x, axes, split_axis=0, concat_axis=0, tiled=True)]
    all_to_all x3 -> x1, waiting for transfers between devices: 19.9 us -> 0.01 us  [exchange(): return lax.all_to_all(x, axes, split_axis=0, concat_axis=0, tiled=True)]
    ppermute x6 -> x22, waiting for transfers between devices: 23.7 us -> 6.23 us  [from_earlier(): lax.ppermute(shard, axes, [(p, (p + k) % count) for p in range(count if w...]
    pallas_call x3 -> x2, Pallas kernels: 14.1 us -> 12.6 us  [the longest x1 7.59 us: mixer_rows(): pl.pallas_call(body, in_specs=[smem, smem] + [vmem] * (8 + len(states)),...]
  transfers between devices with their start and end apart: 9 -> 23, of which waited for: 7 -> 3; matrix products, arithmetic and copies ran while one was open for 0% -> 0% of each run, Pallas kernels for 27% -> 13%
where the time goes in v1:
time: 151 us; the launch traced here: 149 us
  starting transfers between devices  61.6 us (41%)
  blocking collectives  41.6 us (28%)
  Pallas kernels  37.9 us (25%)
  waiting for transfers between devices  6.24 us (4%)
  between operations  1.71 us (1%)
    ppermute x22, starting transfers between devices, from_earlier(): lax.ppermute(shard, axes, [(p, (p + k) % count) for p in range(count if w...  56.8 us
    all_to_all x1, blocking collectives, exchange(): return lax.all_to_all(x, axes, split_axis=0, concat_axis=0, tiled=True)  41.6 us
    pallas_call x1, Pallas kernels, expert_products(): pl.pallas_call(body, in_specs=[pl.BlockSpec(memory_space=pltpu.VMEM), hbm...  10.5 us
    pallas_call x1, Pallas kernels, mixer_rows(): pl.pallas_call(body, in_specs=[smem, smem] + [vmem] * (8 + len(states)),...  7.59 us
    ppermute x22, waiting for transfers between devices, from_earlier(): lax.ppermute(shard, axes, [(p, (p + k) % count) for p in range(count if w...  6.23 us
    pallas_call x1, Pallas kernels, shared_expert(): pl.pallas_call(shared_body, out_shape=pltpu.HBM((tokens, width), F32), co...  5.21 us
    pallas_call x1, Pallas kernels, project(): pl.pallas_call(body, grid=(steps,), in_specs=[pl.BlockSpec(memory_space=p...  4.97 us
    all_to_all x1, starting transfers between devices, exchange(): return lax.all_to_all(x, axes, split_axis=0, concat_axis=0, tiled=True)  4.76 us
  transfers between devices with their start and end apart: 23, of which 3 were waited for; matrix products, arithmetic and copies ran while one was open for 0% of the time, Pallas kernels for 13%

profile of v1, /device:TPU:1, one launch (start us, length us, event | category | flops | bytes accessed | tf_op | source)
XLA Modules:
  0.0 149.1 jit_solution(8827964834228729548)
XLA Ops:
  0.6 4.5 %dispatch_rows.1 = (bf16[1024,1024]{1,0:T(8,128)(2,1)}, bf16[192,2048]{1,0:T(8,128)(2,1)}, s32[8,192]{1,0:T(8,128)}) custom-call(bf16[192,2048]{1,0:T(8,128)(2,1)} %refs_0_.1, f32[1,2048]{1,0:T(1,128)} %bitcast.29, s32[2,192]{1,0:T(2,128)} %bitcast.30), custom_call_target="tpu_custom_call" | custom-call | flops 805306368 | bytes 8388608 | tf_op jit(solution)/shard_map/dispatch_rows/pallas_call | solution.py:102
  5.2 41.6 %all_to_all.10 = bf16[128,8,1024]{2,1,0:T(8,128)(2,1)S(1)} all-to-all(bf16[128,8,1024]{2,1,0:T(8,128)(2,1)} %bitcast.19), channel_id=1, replica_groups=mesh['ep_0'=4,'ep_1'=4,'tp'=8] {'ep_0','ep_1','tp'}, dimensions={0} | all-to-all | bytes 4194304 | tf_op jit(solution)/shard_map/all_to_all | solution.py:503
  46.8 10.5 %expert_products.1 = bf16[64,2,8,1024]{3,2,1,0:T(8,128)(2,1)} custom-call(bf16[64,2,8,1024]{3,2,1,0:T(8,128)(2,1)S(1)} %bitcast.16, bf16[1,2048,1024]{2,1,0:T(8,128)(2,1)} %refs_1_.2, bf16[1,2048,1024]{2,1,0:T(8,128)(2,1)} %refs_2_.1, bf16[1,1024,2048]{2,1,0:T(8,128)(2,1)} %refs_3_.1), custom_call_target="tpu_custom_call" | custom-call | flops 6442450944 | bytes 12582912 | tf_op jit(solution)/shard_map/expert_products/pallas_call | solution.py:202
  57.2 4.8 %all-to-all-start.1 = ((bf16[128,8,1024]{2,1,0:T(8,128)(2,1)}), bf16[128,8,1024]{2,1,0:T(8,128)(2,1)S(1)}, u32[]{:S(2)}, u32[]{:S(2)}) async-start(bf16[128,8,1024]{2,1,0:T(8,128)(2,1)} %bitcast.18), calls=%async_computation.1 | async-start | bytes 4194304 | tf_op jit(solution)/shard_map/all_to_all | solution.py:503
  62.6 1.8 %device_state.1 = f32[72,128]{1,0:T(8,128)S(1)} custom-call(bf16[64,2048]{1,0:T(8,128)(2,1)} %bitcast.20, bf16[2048,128]{1,0:T(8,128)(2,1)} %refs_4_.1, f32[16,128]{1,0:T(8,128)} %bitcast.22, f32[16,128]{1,0:T(8,128)} %bitcast.24, f32[16,128]{1,0:T(8,128)} %bitcast.26, f32[1]{0:T(128)S(6)} %copy.22.bias_ref.refs_1_), custom_call_target="tpu_custom_call" | custom-call | flops 134217728 | bytes 1048576 | tf_op jit(solution)/shard_map/device_state/pallas_call | solution.py:334
  64.5 7.4 %collective-permute-start.14 = (f32[72,128]{1,0:T(8,128)S(1)}, f32[72,128]{1,0:T(8,128)S(1)}, u32[]{:S(2)}, u32[]{:S(2)}) collective-permute-start(f32[72,128]{1,0:T(8,128)S(1)} %device_state.1), channel_id=1, source_target_pairs={{0,120},{1,121},{2,122},{3,123},{4,124},{5,125},{6,126},{7,127}} | collective-permute-start | bytes 110600 | tf_op jit(solution)/shard_map/ppermute | solution.py:509
  71.9 1.3 collective-permute-start.13
  73.2 1.3 collective-permute-start.12
  74.5 1.3 collective-permute-start.11
  75.8 1.3 collective-permute-start.10
  77.1 3.5 %collective-permute-done.14.refs_24_ = f32[72,128]{1,0:T(8,128)S(1)} collective-permute-done((f32[72,128]{1,0:T(8,128)S(1)}, f32[72,128]{1,0:T(8,128)S(1)}, u32[]{:S(2)}, u32[]{:S(2)}) %collective-permute-start.14) | collective-permute-done | bytes 36896 | tf_op jit(solution)/shard_map/ppermute | solution.py:509
  80.6 1.3 collective-permute-start.9
  81.9 1.9 %collective-permute-done.13.refs_23_ = f32[72,128]{1,0:T(8,128)S(1)} collective-permute-done((f32[72,128]{1,0:T(8,128)S(1)}, f32[72,128]{1,0:T(8,128)S(1)}, u32[]{:S(2)}, u32[]{:S(2)}) %collective-permute-start.13) | collective-permute-done | bytes 36896 | tf_op jit(solution)/shard_map/ppermute | solution.py:509
  83.8 1.3 collective-permute-start.8
  85.1 1.3 collective-permute-start.7
  86.4 11.2 %collective-permute-start.6 = (f32[72,128]{1,0:T(8,128)S(1)}, f32[72,128]{1,0:T(8,128)S(1)}, u32[]{:S(2)}, u32[]{:S(2)}) collective-permute-start(f32[72,128]{1,0:T(8,128)S(1)} %device_state.1), channel_id=1, source_target_pairs={{0,56},{8,64},{16,72},{24,80},{32,88},{40,96},{48,104},{56,112},{6... | collective-permute-start | bytes 110600 | tf_op jit(solution)/shard_map/ppermute | solution.py:509
  97.7 2.2 %collective-permute-start.5 = (f32[72,128]{1,0:T(8,128)S(1)}, f32[72,128]{1,0:T(8,128)S(1)}, u32[]{:S(2)}, u32[]{:S(2)}) collective-permute-start(f32[72,128]{1,0:T(8,128)S(1)} %device_state.1), channel_id=1, source_target_pairs={{0,48},{8,56},{16,64},{24,72},{32,80},{40,88},{48,96},{56,104},{64... | collective-permute-start | bytes 110600 | tf_op jit(solution)/shard_map/ppermute | solution.py:509
  99.9 1.3 collective-permute-start.4
  101.2 2.9 %collective-permute-start.3 = (f32[72,128]{1,0:T(8,128)S(1)}, f32[72,128]{1,0:T(8,128)S(1)}, u32[]{:S(2)}, u32[]{:S(2)}) collective-permute-start(f32[72,128]{1,0:T(8,128)S(1)} %device_state.1), channel_id=1, source_target_pairs={{0,32},{8,40},{16,48},{24,56},{32,64},{40,72},{48,80},{56,88},{64,... | collective-permute-start | bytes 110600 | tf_op jit(solution)/shard_map/ppermute | solution.py:509
  104.1 4.3 %collective-permute-start.2 = (f32[72,128]{1,0:T(8,128)S(1)}, f32[72,128]{1,0:T(8,128)S(1)}, u32[]{:S(2)}, u32[]{:S(2)}) collective-permute-start(f32[72,128]{1,0:T(8,128)S(1)} %device_state.1), channel_id=1, source_target_pairs={{0,24},{8,32},{16,40},{24,48},{32,56},{40,64},{48,72},{56,80},{64,... | collective-permute-start | bytes 110600 | tf_op jit(solution)/shard_map/ppermute | solution.py:509
  108.5 1.3 collective-permute-start.1
  109.8 3.3 %collective-permute-start = (f32[72,128]{1,0:T(8,128)S(1)}, f32[72,128]{1,0:T(8,128)S(1)}, u32[]{:S(2)}, u32[]{:S(2)}) collective-permute-start(f32[72,128]{1,0:T(8,128)S(1)} %device_state.1), channel_id=1, source_target_pairs={{0,8},{8,16},{16,24},{24,32},{32,40},{40,48},{48,56},{56,64},{64,7... | collective-permute-start | bytes 110600 | tf_op jit(solution)/shard_map/ppermute | solution.py:509
  114.0 7.6 %mixer_rows.1 = (bf16[272,128]{1,0:T(8,128)(2,1)S(1)}, bf16[272,128]{1,0:T(8,128)(2,1)S(1)}, bf16[272,128]{1,0:T(8,128)(2,1)S(1)}, bf16[272,128]{1,0:T(8,128)(2,...) custom-call(s32[2]{0:T(128)S(1)} %pad_add_fusion.refs_0_, ...), custom_call_target="tpu_custom_call" | custom-call | flops 1073741824 | bytes 2097152 | tf_op jit(solution)/shard_map/mixer_rows/pallas_call | solution.py:441
  121.6 6.3 %collective-permute-start.15 = (bf16[272,128]{1,0:T(8,128)(2,1)S(1)}, bf16[272,128]{1,0:T(8,128)(2,1)S(1)}, u32[]{:S(2)}, u32[]{:S(2)}) collective-permute-start(bf16[272,128]{1,0:T(8,128)(2,1)S(1)} %get-tuple-element.14), channel_id=1, source_target_pairs={{0,1},{1,2},{2,3},{3,4},{4,5},{5,6},{6,7},{7,0},{8,9},{9,10},{10,1... | collective-permute-start | bytes 208904 | tf_op jit(solution)/shard_map/ppermute | solution.py:509
  127.9 1.1 collective-permute-start.16
  129.0 1.4 collective-permute-start.17
  131.2 1.5 collective-permute-start.19
  132.7 0.9 collective-permute-start.20
  133.5 1.9 %collective-permute-start.21 = (bf16[272,128]{1,0:T(8,128)(2,1)S(1)}, bf16[272,128]{1,0:T(8,128)(2,1)S(1)}, u32[]{:S(2)}, u32[]{:S(2)}) collective-permute-start(bf16[272,128]{1,0:T(8,128)(2,1)S(1)} %get-tuple-element.20), channel_id=1, source_target_pairs={{0,7},{1,0},{2,1},{3,2},{4,3},{5,4},{6,5},{7,6},{8,15},{9,8},{10,9... | collective-permute-start | bytes 208904 | tf_op jit(solution)/shard_map/ppermute | solution.py:509
  135.4 5.2 %shared_expert.1.refs_3_ = f32[192,2048]{1,0:T(8,128)} custom-call(bf16[192,2048]{1,0:T(8,128)(2,1)} %get-tuple-element.23.n_ref, bf16[2048,384]{1,0:T(8,128)(2,1)} %g_ref.1, bf16[2048,384]{1,0:T(8,128)(2,1)} %u_ref.1, bf16[384,2048]{1,0:T(8,128)(2,1)} %d_ref.1), custom_call_target="tpu_custom_call" | custom-call | flops 905969664 | bytes 4718592 | tf_op jit(solution)/shard_map/shared_expert/pallas_call | solution.py:234
  140.7 5.0 %project.1 = bf16[256,2048]{1,0:T(8,128)(2,1)} custom-call(s32[2]{0:T(128)S(1)} %pad_add_fusion.refs_0_, bf16[272,128]{1,0:T(8,128)(2,1)S(1)} %get-tuple-element.13.refs_1_, bf16[272,128]{1,0:T(8,128)(2,1)S(1)} %collective-permute-done.15.refs_2_, bf16[272,128]{1,0:T(8,128)(2,1)S(1)} %collective-permute-done.16.refs_3_, ...), custom_call_target="tpu_custom_call" | custom-call | flops 1073741824 | bytes 4194304 | tf_op jit(solution)/shard_map/project/pallas_call | solution.py:487
  145.6 3.3 %combine.1 = bf16[192,2048]{1,0:T(8,128)(2,1)} custom-call(bf16[1024,1024]{1,0:T(8,128)(2,1)S(1)} %bitcast.15, s32[8,192]{1,0:T(8,128)S(1)} %copy-done.1, f32[2,192]{1,0:T(2,128)S(1)} %bitcast.17, f32[192,2048]{1,0:T(8,128)} %shared_expert.1.refs_3_), custom_call_target="tpu_custom_call" | custom-call | flops 1610612736 | bytes 2097152 | tf_op jit(solution)/shard_map/combine/pallas_call | solution.py:276
  (27 shorter events, 1.7 us)
Async XLA Ops:
  57.2 88.4 %all-to-all-start.1 = ((bf16[128,8,1024]{2,1,0:T(8,128)(2,1)}), bf16[128,8,1024]{2,1,0:T(8,128)(2,1)S(1)}, u32[]{:S(2)}, u32[]{:S(2)}) async-start(bf16[128,8,1024]{2,1,0:T(8,128)(2,1)} %bitcast.18), calls=%async_computation.1 | async-start | bytes 4194304 | tf_op jit(solution)/shard_map/all_to_all | solution.py:503
  64.5 16.1 %collective-permute-start.14 = (f32[72,128]{1,0:T(8,128)S(1)}, f32[72,128]{1,0:T(8,128)S(1)}, u32[]{:S(2)}, u32[]{:S(2)}) collective-permute-start(f32[72,128]{1,0:T(8,128)S(1)} %device_state.1), channel_id=1, source_target_pairs={{0,120},{1,121},{2,122},{3,123},{4,124},{5,125},{6,126},{7,127}} | collective-permute-start | bytes 110600 | tf_op jit(solution)/shard_map/ppermute | solution.py:509
  71.9 11.9 %collective-permute-start.13 = (f32[72,128]{1,0:T(8,128)S(1)}, f32[72,128]{1,0:T(8,128)S(1)}, u32[]{:S(2)}, u32[]{:S(2)}) collective-permute-start(f32[72,128]{1,0:T(8,128)S(1)} %device_state.1), channel_id=1, source_target_pairs={{0,112},{8,120},{1,113},{9,121},{2,114},{10,122},{3,115},{11,123},... | collective-permute-start | bytes 110600 | tf_op jit(solution)/shard_map/ppermute | solution.py:509
  73.2 11.9 %collective-permute-start.12 = (f32[72,128]{1,0:T(8,128)S(1)}, f32[72,128]{1,0:T(8,128)S(1)}, u32[]{:S(2)}, u32[]{:S(2)}) collective-permute-start(f32[72,128]{1,0:T(8,128)S(1)} %device_state.1), channel_id=1, source_target_pairs={{0,104},{8,112},{16,120},{1,105},{9,113},{17,121},{2,106},{10,114}... | collective-permute-start | bytes 110600 | tf_op jit(solution)/shard_map/ppermute | solution.py:509
  74.5 11.9 %collective-permute-start.11 = (f32[72,128]{1,0:T(8,128)S(1)}, f32[72,128]{1,0:T(8,128)S(1)}, u32[]{:S(2)}, u32[]{:S(2)}) collective-permute-start(f32[72,128]{1,0:T(8,128)S(1)} %device_state.1), channel_id=1, source_target_pairs={{0,96},{8,104},{16,112},{24,120},{1,97},{9,105},{17,113},{25,121},... | collective-permute-start | bytes 110600 | tf_op jit(solution)/shard_map/ppermute | solution.py:509
  75.8 21.8 %collective-permute-start.10 = (f32[72,128]{1,0:T(8,128)S(1)}, f32[72,128]{1,0:T(8,128)S(1)}, u32[]{:S(2)}, u32[]{:S(2)}) collective-permute-start(f32[72,128]{1,0:T(8,128)S(1)} %device_state.1), channel_id=1, source_target_pairs={{0,88},{8,96},{16,104},{24,112},{32,120},{1,89},{9,97},{17,105},{2... | collective-permute-start | bytes 110600 | tf_op jit(solution)/shard_map/ppermute | solution.py:509
  80.6 19.3 %collective-permute-start.9 = (f32[72,128]{1,0:T(8,128)S(1)}, f32[72,128]{1,0:T(8,128)S(1)}, u32[]{:S(2)}, u32[]{:S(2)}) collective-permute-start(f32[72,128]{1,0:T(8,128)S(1)} %device_state.1), channel_id=1, source_target_pairs={{0,80},{8,88},{16,96},{24,104},{32,112},{40,120},{1,81},{9,89},{17... | collective-permute-start | bytes 110600 | tf_op jit(solution)/shard_map/ppermute | solution.py:509
  83.8 17.3 %collective-permute-start.8 = (f32[72,128]{1,0:T(8,128)S(1)}, f32[72,128]{1,0:T(8,128)S(1)}, u32[]{:S(2)}, u32[]{:S(2)}) collective-permute-start(f32[72,128]{1,0:T(8,128)S(1)} %device_state.1), channel_id=1, source_target_pairs={{0,72},{8,80},{16,88},{24,96},{32,104},{40,112},{48,120},{1,73},{9... | collective-permute-start | bytes 110600 | tf_op jit(solution)/shard_map/ppermute | solution.py:509
  85.1 19.0 %collective-permute-start.7 = (f32[72,128]{1,0:T(8,128)S(1)}, f32[72,128]{1,0:T(8,128)S(1)}, u32[]{:S(2)}, u32[]{:S(2)}) collective-permute-start(f32[72,128]{1,0:T(8,128)S(1)} %device_state.1), channel_id=1, source_target_pairs={{0,64},{8,72},{16,80},{24,88},{32,96},{40,104},{48,112},{56,120},{... | collective-permute-start | bytes 110600 | tf_op jit(solution)/shard_map/ppermute | solution.py:509
  86.4 22.0 %collective-permute-start.6 = (f32[72,128]{1,0:T(8,128)S(1)}, f32[72,128]{1,0:T(8,128)S(1)}, u32[]{:S(2)}, u32[]{:S(2)}) collective-permute-start(f32[72,128]{1,0:T(8,128)S(1)} %device_state.1), channel_id=1, source_target_pairs={{0,56},{8,64},{16,72},{24,80},{32,88},{40,96},{48,104},{56,112},{6... | collective-permute-start | bytes 110600 | tf_op jit(solution)/shard_map/ppermute | solution.py:509
  97.7 12.1 %collective-permute-start.5 = (f32[72,128]{1,0:T(8,128)S(1)}, f32[72,128]{1,0:T(8,128)S(1)}, u32[]{:S(2)}, u32[]{:S(2)}) collective-permute-start(f32[72,128]{1,0:T(8,128)S(1)} %device_state.1), channel_id=1, source_target_pairs={{0,48},{8,56},{16,64},{24,72},{32,80},{40,88},{48,96},{56,104},{64... | collective-permute-start | bytes 110600 | tf_op jit(solution)/shard_map/ppermute | solution.py:509
  99.9 13.3 %collective-permute-start.4 = (f32[72,128]{1,0:T(8,128)S(1)}, f32[72,128]{1,0:T(8,128)S(1)}, u32[]{:S(2)}, u32[]{:S(2)}) collective-permute-start(f32[72,128]{1,0:T(8,128)S(1)} %device_state.1), channel_id=1, source_target_pairs={{0,40},{8,48},{16,56},{24,64},{32,72},{40,80},{48,88},{56,96},{64,... | collective-permute-start | bytes 110600 | tf_op jit(solution)/shard_map/ppermute | solution.py:509
  101.2 12.0 %collective-permute-start.3 = (f32[72,128]{1,0:T(8,128)S(1)}, f32[72,128]{1,0:T(8,128)S(1)}, u32[]{:S(2)}, u32[]{:S(2)}) collective-permute-start(f32[72,128]{1,0:T(8,128)S(1)} %device_state.1), channel_id=1, source_target_pairs={{0,32},{8,40},{16,48},{24,56},{32,64},{40,72},{48,80},{56,88},{64,... | collective-permute-start | bytes 110600 | tf_op jit(solution)/shard_map/ppermute | solution.py:509
  104.1 9.1 %collective-permute-start.2 = (f32[72,128]{1,0:T(8,128)S(1)}, f32[72,128]{1,0:T(8,128)S(1)}, u32[]{:S(2)}, u32[]{:S(2)}) collective-permute-start(f32[72,128]{1,0:T(8,128)S(1)} %device_state.1), channel_id=1, source_target_pairs={{0,24},{8,32},{16,40},{24,48},{32,56},{40,64},{48,72},{56,80},{64,... | collective-permute-start | bytes 110600 | tf_op jit(solution)/shard_map/ppermute | solution.py:509
  108.5 4.7 %collective-permute-start.1 = (f32[72,128]{1,0:T(8,128)S(1)}, f32[72,128]{1,0:T(8,128)S(1)}, u32[]{:S(2)}, u32[]{:S(2)}) collective-permute-start(f32[72,128]{1,0:T(8,128)S(1)} %device_state.1), channel_id=1, source_target_pairs={{0,16},{8,24},{16,32},{24,40},{32,48},{40,56},{48,64},{56,72},{64,... | collective-permute-start | bytes 110600 | tf_op jit(solution)/shard_map/ppermute | solution.py:509
  109.8 4.2 %collective-permute-start = (f32[72,128]{1,0:T(8,128)S(1)}, f32[72,128]{1,0:T(8,128)S(1)}, u32[]{:S(2)}, u32[]{:S(2)}) collective-permute-start(f32[72,128]{1,0:T(8,128)S(1)} %device_state.1), channel_id=1, source_target_pairs={{0,8},{8,16},{16,24},{24,32},{32,40},{40,48},{48,56},{56,64},{64,7... | collective-permute-start | bytes 110600 | tf_op jit(solution)/shard_map/ppermute | solution.py:509
  121.6 11.1 %collective-permute-start.15 = (bf16[272,128]{1,0:T(8,128)(2,1)S(1)}, bf16[272,128]{1,0:T(8,128)(2,1)S(1)}, u32[]{:S(2)}, u32[]{:S(2)}) collective-permute-start(bf16[272,128]{1,0:T(8,128)(2,1)S(1)} %get-tuple-element.14), channel_id=1, source_target_pairs={{0,1},{1,2},{2,3},{3,4},{4,5},{5,6},{6,7},{7,0},{8,9},{9,10},{10,1... | collective-permute-start | bytes 208904 | tf_op jit(solution)/shard_map/ppermute | solution.py:509
  127.9 5.7 %collective-permute-start.16 = (bf16[272,128]{1,0:T(8,128)(2,1)S(1)}, bf16[272,128]{1,0:T(8,128)(2,1)S(1)}, u32[]{:S(2)}, u32[]{:S(2)}) collective-permute-start(bf16[272,128]{1,0:T(8,128)(2,1)S(1)} %get-tuple-element.15), channel_id=1, source_target_pairs={{0,2},{1,3},{2,4},{3,5},{4,6},{5,7},{6,0},{7,1},{8,10},{9,11},{10,... | collective-permute-start | bytes 208904 | tf_op jit(solution)/shard_map/ppermute | solution.py:509
  129.0 11.6 %collective-permute-start.17 = (bf16[272,128]{1,0:T(8,128)(2,1)S(1)}, bf16[272,128]{1,0:T(8,128)(2,1)S(1)}, u32[]{:S(2)}, u32[]{:S(2)}) collective-permute-start(bf16[272,128]{1,0:T(8,128)(2,1)S(1)} %get-tuple-element.16), channel_id=1, source_target_pairs={{0,3},{1,4},{2,5},{3,6},{4,7},{5,0},{6,1},{7,2},{8,11},{9,12},{10,... | collective-permute-start | bytes 208904 | tf_op jit(solution)/shard_map/ppermute | solution.py:509
  130.4 10.2 %collective-permute-start.18 = (bf16[272,128]{1,0:T(8,128)(2,1)S(1)}, bf16[272,128]{1,0:T(8,128)(2,1)S(1)}, u32[]{:S(2)}, u32[]{:S(2)}) collective-permute-start(bf16[272,128]{1,0:T(8,128)(2,1)S(1)} %get-tuple-element.17), channel_id=1, source_target_pairs={{0,4},{1,5},{2,6},{3,7},{4,0},{5,1},{6,2},{7,3},{8,12},{9,13},{10,... | collective-permute-start | bytes 208904 | tf_op jit(solution)/shard_map/ppermute | solution.py:509
  131.2 9.4 %collective-permute-start.19 = (bf16[272,128]{1,0:T(8,128)(2,1)S(1)}, bf16[272,128]{1,0:T(8,128)(2,1)S(1)}, u32[]{:S(2)}, u32[]{:S(2)}) collective-permute-start(bf16[272,128]{1,0:T(8,128)(2,1)S(1)} %get-tuple-element.18), channel_id=1, source_target_pairs={{0,5},{1,6},{2,7},{3,0},{4,1},{5,2},{6,3},{7,4},{8,13},{9,14},{10,... | collective-permute-start | bytes 208904 | tf_op jit(solution)/shard_map/ppermute | solution.py:509
  132.7 8.0 %collective-permute-start.20 = (bf16[272,128]{1,0:T(8,128)(2,1)S(1)}, bf16[272,128]{1,0:T(8,128)(2,1)S(1)}, u32[]{:S(2)}, u32[]{:S(2)}) collective-permute-start(bf16[272,128]{1,0:T(8,128)(2,1)S(1)} %get-tuple-element.19), channel_id=1, source_target_pairs={{0,6},{1,7},{2,0},{3,1},{4,2},{5,3},{6,4},{7,5},{8,14},{9,15},{10,... | collective-permute-start | bytes 208904 | tf_op jit(solution)/shard_map/ppermute | solution.py:509
  133.5 7.1 %collective-permute-start.21 = (bf16[272,128]{1,0:T(8,128)(2,1)S(1)}, bf16[272,128]{1,0:T(8,128)(2,1)S(1)}, u32[]{:S(2)}, u32[]{:S(2)}) collective-permute-start(bf16[272,128]{1,0:T(8,128)(2,1)S(1)} %get-tuple-element.20), channel_id=1, source_target_pairs={{0,7},{1,0},{2,1},{3,2},{4,3},{5,4},{6,5},{7,6},{8,15},{9,8},{10,9... | collective-permute-start | bytes 208904 | tf_op jit(solution)/shard_map/ppermute | solution.py:509
  140.6 5.0 %copy-start = (f32[192,2]{0,1:T(2,128)S(1)}, f32[192,2]{0,1:T(2,128)}, u32[]{:S(2)}) copy-start(f32[192,2]{0,1:T(2,128)} %param.33) | copy-start | bytes 4612
  140.7 5.0 %copy-start.1 = (s32[8,192]{1,0:T(8,128)S(1)}, s32[8,192]{1,0:T(8,128)}, u32[]{:S(2)}) copy-start(s32[8,192]{1,0:T(8,128)} %get-tuple-element.22.refs_1_) | copy-start | bytes 18436

commit v2 on v0

--- a/solution.py
+++ b/solution.py
@@ -34,10 +34,6 @@
     return lax.broadcasted_iota(jnp.int32, shape, dim)
 
 
-def whole(shape):
-    return pl.BlockSpec(shape, lambda *_: (0,) * len(shape))
-
-
 def params(mib, grid=False):
     return pltpu.CompilerParams(
         vmem_limit_bytes=mib * 2**20,
@@ -53,7 +49,7 @@
     return pl.CostEstimate(flops=int(flops), bytes_accessed=int(nbytes), transcendentals=0)
 
 
-def slot_rows(idx, cap, experts):
+def copy_slots(idx, cap, experts):
     tokens = idx.shape[1]
     sub = iota((experts, tokens), 0)
     first = sub == idx[0:1, :]
@@ -62,60 +58,79 @@
     before = jnp.where(iota((tokens, tokens), 0) < iota((tokens, tokens), 1), 1.0, 0.0)
     prior = dot(named, before.astype(BF16))
     places = [jnp.sum(jnp.where(hot, prior, 0.0), axis=0, keepdims=True) for hot in (first, second)]
-    return [
-        idx[j : j + 1, :] * (2 * cap) + places[j].astype(jnp.int32) for j in range(2)
-    ]
-
-
-def dispatch_body(cap, experts, x_ref, gain_ref, idx_ref, send_ref, normed_ref, rows_ref, both_ref, want_ref):
-    step = pl.program_id(0)
+    return [idx[j : j + 1, :] * cap + places[j].astype(jnp.int32) for j in range(2)]
+
+
+def dispatch_body(
+    cap, x_hbm, gain_hbm, idx_hbm, send_hbm, normed_hbm, slots_hbm,
+    x_ref, gain_ref, idx_ref, send_ref, normed_ref, slots_ref, in_sems, out_sems,
+):
     tokens, width = x_ref.shape
     half = width // 2
-
-    @pl.when(step == 0)
-    def _():
-        x = x_ref[...].astype(F32)
-        scale = lax.rsqrt(jnp.mean(x * x, axis=-1, keepdims=True) + 1e-06)
-        normed = (x * scale * gain_ref[...]).astype(BF16)
-        normed_ref[...] = normed
-        both_ref[0:tokens, :] = normed[:, :half]
-        both_ref[tokens:, :] = normed[:, half:]
-        row0, row1 = slot_rows(idx_ref[...], cap, experts)
-        rows_ref[...] = jnp.concatenate([row0, row1, row0, row1, row0, row1, row0, row1], axis=0)
-        want_ref[0:1, 0:tokens] = row0
-        want_ref[1:2, 0:tokens] = row1
-
-    rows = send_ref.shape[0]
-    row = iota((rows, tokens), 0) + step * rows
-    t0, t1 = want_ref[0:1, 0:tokens], want_ref[1:2, 0:tokens]
-    low = jnp.where((row == t0) | (row == t1), 1.0, 0.0).astype(BF16)
-    high = jnp.where((row == t0 + cap) | (row == t1 + cap), 1.0, 0.0).astype(BF16)
-    out = dot(low, both_ref[0:tokens, :]) + dot(high, both_ref[tokens:, :])
-    send_ref[...] = out.astype(BF16)
+    pieces, pairs = send_ref.shape[0:2]
+    experts = 2 * pieces * pairs
+    loads = [
+        pltpu.make_async_copy(src, dst, in_sems.at[i])
+        for i, (src, dst) in enumerate(((idx_hbm, idx_ref), (gain_hbm, gain_ref), (x_hbm, x_ref)))
+    ]
+    for load in loads:
+        load.start()
+    loads[0].wait()
+    slot0, slot1 = copy_slots(idx_ref[...], cap, experts)
+    slots_ref[...] = jnp.concatenate([slot0, slot1] * 4, axis=0)
+    stores = [pltpu.make_async_copy(slots_ref, slots_hbm, out_sems.at[pieces])]
+    stores[0].start()
+    loads[1].wait()
+    loads[2].wait()
+    x = x_ref[...].astype(F32)
+    scale = lax.rsqrt(jnp.mean(x * x, axis=-1, keepdims=True) + 1e-06)
+    normed = (x * scale * gain_ref[...]).astype(BF16)
+    normed_ref[...] = normed
+    lower = iota((pairs, 8, half), 1) < 4
+    rows = pairs * 2 * cap
+    for p in range(pieces):
+        row = iota((rows, tokens), 0) + p * rows
+        wanted = jnp.where((row == slot0) | (row == slot1), 1.0, 0.0).astype(BF16)
+        first = dot(wanted, normed_ref[:, :half]).reshape(pairs, 8, half)
+        last = dot(wanted, normed_ref[:, half:]).reshape(pairs, 8, half)
+        even, odd = swap_halves(first, last, lower)
+        send_ref[p, :, 0] = even.astype(BF16)
+        send_ref[p, :, 1] = odd.astype(BF16)
+        stores.append(pltpu.make_async_copy(send_ref.at[p], send_hbm.at[p], out_sems.at[p]))
+        stores[-1].start()
+    stores.append(pltpu.make_async_copy(normed_ref, normed_hbm, out_sems.at[pieces + 1]))
+    stores[-1].start()
+    for store in stores:
+        store.wait()
 
 
 def dispatch_rows(x, gain, idx, cap, experts):
     tokens, width = x.shape
-    total = experts * cap * 2
-    steps = 4
-    body = lambda *refs: dispatch_body(cap, experts, *refs)
+    pieces = 4
+    shape = (pieces, experts // (2 * pieces), 2, 2 * cap, width // 2)
+    hbm = pl.BlockSpec(memory_space=pltpu.HBM)
+    body = lambda *refs: dispatch_body(cap, *refs)
     return pl.pallas_call(
         body,
-        grid=(steps,),
-        in_specs=[whole((tokens, width)), whole((1, width)), whole((2, tokens))],
-        out_specs=[
-            pl.BlockSpec((total // steps, width // 2), lambda i: (i, 0)),
-            whole((tokens, width)),
-            whole((8, tokens)),
-        ],
+        in_specs=[hbm] * 3,
+        out_specs=[hbm] * 3,
         out_shape=[
-            pltpu.HBM((total, width // 2), BF16),
+            pltpu.HBM(shape, BF16),
             pltpu.HBM((tokens, width), BF16),
             pltpu.HBM((8, tokens), jnp.int32),
         ],
-        scratch_shapes=[pltpu.VMEM((2 * tokens, width // 2), BF16), pltpu.VMEM((8, 256), jnp.int32)],
-        compiler_params=params(20, True),
-        cost_estimate=cost(2 * total * tokens * width, 4 * total * width),
+        scratch_shapes=[
+            pltpu.VMEM((tokens, width), BF16),
+            pltpu.VMEM((1, width), F32),
+            pltpu.VMEM((2, tokens), jnp.int32),
+            pltpu.VMEM(shape, BF16),
+            pltpu.VMEM((tokens, width), BF16),
+            pltpu.VMEM((8, tokens), jnp.int32),
+            pltpu.SemaphoreType.DMA((3,)),
+            pltpu.SemaphoreType.DMA((pieces + 2,)),
+        ],
+        compiler_params=params(20),
+        cost_estimate=cost(2 * experts * cap * tokens * width, 4 * experts * cap * width),
         name="dispatch_rows",
     )(*in_hbm(x, gain, idx))
 
@@ -151,9 +166,7 @@
             ]
         )
         stores.append(pltpu.make_async_copy(o_ref.at[p], out_hbm.at[:, :, :, at], sems.at[4, p]))
-    loads = first_loads + last_loads
-    ahead = 3
-    for copies in loads[:ahead]:
+    for copies in first_loads + last_loads:
         for copy in copies:
             copy.start()
     lower = iota((group, 8, half), 1) < 4
@@ -164,22 +177,17 @@
         x_ref[at, 0:half] = first.reshape(group * 8, half).astype(BF16)
         x_ref[at, half:] = last.reshape(group * 8, half).astype(BF16)
 
-    def arrive(n):
-        for copy in loads[n]:
+    for p in range(pieces):
+        for copy in first_loads[p]:
             copy.wait()
-        if n + ahead < len(loads):
-            for copy in loads[n + ahead]:
-                copy.start()
-
-    for p in range(pieces):
-        arrive(p)
         x = x_ref[...]
         gate = dot(x, g_ref[p])
         up = dot(x, u_ref[p])
         h_ref[:, p * wide : (p + 1) * wide] = (gate * jax.nn.sigmoid(gate) * up).astype(BF16)
     lower = iota((pairs, 8, part), 1) < 4
     for p in range(pieces):
-        arrive(pieces + p)
+        for copy in last_loads[p]:
+            copy.wait()
         h = h_ref[...]
         first = dot(h, d_ref[p, 0]).reshape(pairs, 8, part)
         last = dot(h, d_ref[p, 1]).reshape(pairs, 8, part)
@@ -240,7 +248,9 @@
     )(*in_hbm(normed, gate_weight, up_weight, down_weight))
 
 
-def combine_body(cap, back_ref, rows_ref, weight_ref, shared_hbm, out_hbm, shared_ref, out_ref, sems):
+def combine_body(
+    cap, back_ref, slots_ref, weight_ref, shared_hbm, w_hbm, out_hbm, w_ref, shared_ref, out_ref, sems, w_sem
+):
     tokens, _ = out_ref.shape
     total, half = back_ref.shape
     loads, stores = [], []
@@ -251,42 +261,51 @@
         )
         stores.append(pltpu.make_async_copy(out_ref.at[:, cols], out_hbm.at[:, cols], sems.at[1, h]))
         loads[h].start()
-    row_col = jnp.transpose(rows_ref[...].astype(F32))
-    weight_col = jnp.transpose(jnp.concatenate([weight_ref[...]] * 4, axis=0))
-    at0, at1 = row_col[:, 0:1].astype(jnp.int32), row_col[:, 1:2].astype(jnp.int32)
-    w0, w1 = weight_col[:, 0:1], weight_col[:, 1:2]
+    bring = pltpu.make_async_copy(w_hbm, w_ref, w_sem)
+    bring.start()
+    slot_col = jnp.transpose(slots_ref[...].astype(F32)).astype(jnp.int32)
+    weight_col = jnp.transpose(jnp.concatenate([weight_ref[...]] * 4, axis=0)).astype(BF16)
     lane = iota((tokens, total), 1)
+    at = [(s // cap) * (2 * cap) + s % cap for s in (slot_col[:, 0:1], slot_col[:, 1:2])]
     for h in range(2):
         cols = slice(h * half, (h + 1) * half)
-        mixed = jnp.where(lane == at0 + h * cap, w0, jnp.where(lane == at1 + h * cap, w1, 0.0))
-        product = dot(jnp.concatenate(split_two(mixed), axis=0), back_ref[...])
+        mix = jnp.where(
+            lane == at[0] + h * cap,
+            weight_col[:, 0:1].astype(F32),
+            jnp.where(lane == at[1] + h * cap, weight_col[:, 1:2].astype(F32), 0.0),
+        ).astype(BF16)
+        routed = dot(mix, back_ref[...])
         loads[h].wait()
-        routed = product[0:tokens] + product[tokens:]
         out_ref[:, cols] = (routed + shared_ref[:, cols]).astype(BF16)
         stores[h].start()
     for store in stores:
         store.wait()
-
-
-def combine(back, rows, weights, shared, cap):
+    bring.wait()
+
+
+def combine(back, slots, weights, shared, cap, mixer_weight):
     tokens, width = shared.shape
     hbm = pl.BlockSpec(memory_space=pltpu.HBM)
     vmem = pl.BlockSpec(memory_space=pltpu.VMEM)
     body = lambda *refs: combine_body(cap, *refs)
     return pl.pallas_call(
         body,
-        in_specs=[vmem, vmem, vmem, hbm],
-        out_specs=hbm,
-        out_shape=jax.ShapeDtypeStruct((tokens, width), BF16),
+        in_specs=[vmem, vmem, vmem, hbm, hbm],
+        out_specs=[hbm, vmem],
+        out_shape=[
+            jax.ShapeDtypeStruct((tokens, width), BF16),
+            pltpu.VMEM(mixer_weight.shape, BF16),
+        ],
         scratch_shapes=[
             pltpu.VMEM((tokens, width), F32),
             pltpu.VMEM((tokens, width), BF16),
             pltpu.SemaphoreType.DMA((2, 2)),
+            pltpu.SemaphoreType.DMA,
         ],
         compiler_params=params(20),
         cost_estimate=cost(4 * tokens * back.shape[0] * width, 2 * back.size),
         name="combine",
-    )(back, rows, weights, *in_hbm(shared))
+    )(back, slots, weights, *in_hbm(shared, mixer_weight))
 
 
 def gate_rows(in_ref, forget_ref, extra_ref, bias_ref):
@@ -428,8 +447,8 @@
     blocks = length // BLK
     rows = list(refs[:rows_count])
     columns = list(refs[rows_count : rows_count + columns_count])
-    out_ref = refs[-1]
-    peers = out_ref.shape[0]
+    *outs, out_ref = refs[rows_count + columns_count :]
+    peers = len(outs)
     tokens = length // peers
     per_chunk = tokens // BLK
     in_gate, cumulative, total = gate_rows(in_ref, forget_ref, extra_ref, bias_ref)
@@ -480,6 +499,8 @@
         rows = [hi.astype(F32) for hi, _ in parts] + [lo.astype(F32) for _, lo in parts]
         rows.append(jnp.zeros((16 - len(rows), BLK), F32))
         out_ref[c, tokens:, :] = jnp.concatenate(rows, axis=0).astype(BF16)
+    for k in range(peers):
+        outs[k][...] = out_ref[(place_ref[2] + k) % peers]
 
 
 def mixer_rows(place, bias, rows, columns, queries, keys, values, in_gate, forget, extra, gate, gain, peers):
@@ -491,7 +512,8 @@
     return pl.pallas_call(
         body,
         in_specs=[smem, smem] + [vmem] * (8 + len(rows) + len(columns)),
-        out_shape=pltpu.HBM((peers, *chunk), BF16),
+        out_shape=[jax.ShapeDtypeStruct(chunk, BF16)] * peers,
+        scratch_shapes=[pltpu.VMEM((peers, *chunk), BF16)],
         compiler_params=params(16),
         cost_estimate=cost(32 * length * BLK * BLK, 8 * length * BLK),
         name="mixer_rows",
@@ -504,56 +526,66 @@
     )
 
 
-def project_body(g_ref, w_ref, out_ref, scale_ref):
-    heads = g_ref.shape[0]
-    tokens = out_ref.shape[0]
+def project_body(heads, place_ref, *refs):
+    chunks = refs[:heads]
+    w_ref, out_hbm, all_ref, out_ref, sems = refs[heads:]
+    pieces, tokens, wide = out_ref.shape
     per_chunk = tokens // BLK
-
-    @pl.when(pl.program_id(0) == 0)
-    def _():
-        tail = g_ref[0, tokens:, :].astype(F32)
-        for h in range(1, heads):
-            tail = tail + g_ref[h, tokens:, :].astype(F32)
-        for c in range(per_chunk):
-            row = tail[c : c + 1, :] + tail[per_chunk + c : per_chunk + c + 1, :]
-            row = lax.rsqrt(row / (heads * BLK) + 1e-06)
-            scale_ref[c * BLK : (c + 1) * BLK, :] = jnp.transpose(jnp.broadcast_to(row, (BLK, BLK)))
-
-    mixed = jnp.concatenate([g_ref[h, 0:tokens, :] for h in range(heads)], axis=1)
-    product = dot(mixed, w_ref[...])
-    out_ref[...] = (product * scale_ref[:, 0:1]).astype(BF16)
-
-
-def project(gathered, weight):
-    _, rows, _ = gathered.shape
+    for k in range(heads):
+        all_ref[(place_ref[2] + heads - k) % heads] = chunks[k][0:tokens, :]
+    tail = chunks[0][tokens:, :].astype(F32)
+    for k in range(1, heads):
+        tail = tail + chunks[k][tokens:, :].astype(F32)
+    scales = []
+    for c in range(per_chunk):
+        row = tail[c : c + 1, :] + tail[per_chunk + c : per_chunk + c + 1, :]
+        row = lax.rsqrt(row / (heads * BLK) + 1e-06)
+        scales.append(jnp.transpose(jnp.broadcast_to(row, (BLK, BLK)))[:, 0:1])
+    scale = jnp.concatenate(scales, axis=0)
+    mixed = jnp.concatenate([all_ref[h] for h in range(heads)], axis=1)
+    stores = []
+    for p in range(pieces):
+        at = slice(p * wide, (p + 1) * wide)
+        out_ref[p] = (dot(mixed, w_ref[:, at]) * scale).astype(BF16)
+        stores.append(pltpu.make_async_copy(out_ref.at[p], out_hbm.at[:, at], sems.at[p]))
+        stores[p].start()
+    for store in stores:
+        store.wait()
+
+
+def project(place, chunks, weight):
+    heads = len(chunks)
+    rows = chunks[0].shape[0]
     tokens = rows - 16
     width = weight.shape[1]
-    steps = 4
+    pieces = 4
+    vmem = pl.BlockSpec(memory_space=pltpu.VMEM)
+    body = lambda *refs: project_body(heads, *refs)
     return pl.pallas_call(
-        project_body,
-        grid=(steps,),
-        in_specs=[
-            whole(gathered.shape),
-            pl.BlockSpec((weight.shape[0], width // steps), lambda i: (0, i)),
+        body,
+        in_specs=[pl.BlockSpec(memory_space=pltpu.SMEM)] + [vmem] * (heads + 1),
+        out_specs=pl.BlockSpec(memory_space=pltpu.HBM),
+        out_shape=jax.ShapeDtypeStruct((tokens, width), BF16),
+        scratch_shapes=[
+            pltpu.VMEM((heads, tokens, BLK), BF16),
+            pltpu.VMEM((pieces, tokens, width // pieces), BF16),
+            pltpu.SemaphoreType.DMA((pieces,)),
         ],
-        out_specs=pl.BlockSpec((tokens, width // steps), lambda i: (0, i)),
-        out_shape=jax.ShapeDtypeStruct((tokens, width), BF16),
-        scratch_shapes=[pltpu.VMEM((tokens, BLK), F32)],
-        compiler_params=params(16, True),
+        compiler_params=params(16),
         cost_estimate=cost(2 * tokens * weight.size, 2 * weight.size),
         name="project",
-    )(gathered, *in_hbm(weight))
+    )(place, *chunks, weight)
 
 
 def exchange(x, axes):
     return lax.all_to_all(x, axes, split_axis=0, concat_axis=0, tiled=True)
 
 
-def from_earlier(x, axis):
+def from_earlier(shards, axis):
     count = lax.axis_size(axis)
     return [
-        lax.ppermute(x, axis, [(p, (p + k) % count) for p in range(count)])
-        for k in range(1, count)
+        lax.ppermute(shard, axis, [(p, (p + k) % count) for p in range(count)])
+        for k, shard in enumerate(shards, 1)
     ]
 
 
@@ -583,7 +615,7 @@
     ep_count, tp_count = lax.axis_size(EP), lax.axis_size("tp")
     experts = ep_count * tp_count
     cap = 4
-    send, normed, rows = dispatch_rows(
+    send, normed, slots = dispatch_rows(
         second_batch_input, expert_norm_gain[None, :], routed_expert_index.T, cap, experts
     )
     landed = exchange(send.reshape(experts, 2 * cap, -1), EP_TP)
@@ -599,10 +631,10 @@
     query_rows, key_rows = queries.T, head_key_rows.T
     place = jnp.stack([lax.axis_index(a).astype(jnp.int32) for a in ("ep_0", "ep_1", "tp")])
     own = device_state(key_rows, head_value_rows, in_gate, forget, extra, head_forget_bias)
-    row_states = [own] + from_earlier(own, "ep_1")
+    row_states = [own] + from_earlier([own] * (lax.axis_size("ep_1") - 1), "ep_1")
     row_total = row_state(place, row_states)
-    column_states = from_earlier(row_total, "ep_0")
-    mixed = mixer_rows(
+    column_states = from_earlier([row_total] * (lax.axis_size("ep_0") - 1), "ep_0")
+    chunks = mixer_rows(
         place,
         head_forget_bias,
         row_states,
@@ -618,13 +650,18 @@
         tp_count,
     )
     shared = shared_expert(normed, shared_gate_weight, shared_up_weight, shared_down_weight)
-    gathered = exchange(mixed, "tp")
+    gathered = [chunks[0]] + from_earlier(chunks[1:], "tp")
     produced = expert_products(landed, routed_gate_weight, routed_up_weight, routed_down_weight)
     back = exchange(produced, EP_TP)
-    mixer_first_output = project(gathered, mixer_output_weight)
-    moe_out = combine(
-        back.reshape(experts * 2 * cap, -1), rows, routed_copy_weight.T, shared, cap
-    )
+    moe_out, near_weight = combine(
+        back.reshape(experts * 2 * cap, -1),
+        slots,
+        routed_copy_weight.T,
+        shared,
+        cap,
+        mixer_output_weight,
+    )
+    mixer_first_output = project(place, gathered, near_weight)
     return (mixer_first_output, moe_out)
 
 

time: 118 us -> 127 us (1.076)
  blocking collectives: 0 us -> 41.6 us
  waiting for transfers between devices: 43.6 us -> 23.8 us
  starting transfers between devices: 32.8 us -> 24.3 us
  Pallas kernels: 39.4 us -> 35.2 us
    all_to_all x0 -> x1, blocking collectives: none -> 41.6 us  [exchange(): return lax.all_to_all(x, axes, split_axis=0, concat_axis=0, tiled=True)]
    all_to_all x3 -> x1, starting transfers between devices: 25 us -> 4.76 us  [exchange(): return lax.all_to_all(x, axes, split_axis=0, concat_axis=0, tiled=True)]
    all_to_all x3 -> x1, waiting for transfers between devices: 19.9 us -> 0.01 us  [exchange(): return lax.all_to_all(x, axes, split_axis=0, concat_axis=0, tiled=True)]
    ppermute x6 -> x13, starting transfers between devices: 7.81 us -> 19.5 us  [from_earlier(): lax.ppermute(shard, axis, [(p, (p + k) % count) for p in range(count)])]
    pallas_call x3, Pallas kernels: 12.8 us -> 9.26 us  [the longest x1 3.46 us: dispatch_rows(): pl.pallas_call(body, in_specs=[hbm] * 3, out_specs=[hbm] * 3, out_shape=[...]
    ppermute x6 -> x13, waiting for transfers between devices: 23.7 us -> 23.8 us  [from_earlier(): lax.ppermute(shard, axis, [(p, (p + k) % count) for p in range(count)])]
  transfers between devices with their start and end apart: 9 -> 14, of which waited for: 7 -> 6; matrix products, arithmetic and copies ran while one was open for 0% -> 0% of each run, Pallas kernels for 27% -> 15%
where the time goes in v2:
time: 127 us; the launch traced here: 126 us
  blocking collectives  41.6 us (33%)
  Pallas kernels  35.2 us (28%)
  starting transfers between devices  24.3 us (19%)
  waiting for transfers between devices  23.8 us (19%)
  between operations  1.54 us (1%)
    all_to_all x1, blocking collectives, exchange(): return lax.all_to_all(x, axes, split_axis=0, concat_axis=0, tiled=True)  41.6 us
    ppermute x13, waiting for transfers between devices, from_earlier(): lax.ppermute(shard, axis, [(p, (p + k) % count) for p in range(count)])  23.8 us
    ppermute x13, starting transfers between devices, from_earlier(): lax.ppermute(shard, axis, [(p, (p + k) % count) for p in range(count)])  19.5 us
    pallas_call x1, Pallas kernels, expert_products(): pl.pallas_call(body, in_specs=[pl.BlockSpec(memory_space=pltpu.VMEM), hbm...  10.5 us
    pallas_call x1, Pallas kernels, mixer_rows(): pl.pallas_call(body, in_specs=[smem, smem] + [vmem] * (8 + len(rows) + le...  7.59 us
    pallas_call x1, Pallas kernels, shared_expert(): pl.pallas_call(shared_body, out_shape=pltpu.HBM((tokens, width), F32), co...  5.25 us
    all_to_all x1, starting transfers between devices, exchange(): return lax.all_to_all(x, axes, split_axis=0, concat_axis=0, tiled=True)  4.76 us
    pallas_call x1, Pallas kernels, dispatch_rows(): pl.pallas_call(body, in_specs=[hbm] * 3, out_specs=[hbm] * 3, out_shape=[...  3.46 us
  transfers between devices with their start and end apart: 14, of which 6 were waited for; matrix products, arithmetic and copies ran while one was open for 0% of the time, Pallas kernels for 15%

profile of v2, /device:TPU:1, one launch (start us, length us, event | category | flops | bytes accessed | tf_op | source)
XLA Modules:
  0.0 126.5 jit_solution(7446461022798265823)
XLA Ops:
  0.6 3.5 %dispatch_rows.1 = (bf16[4,16,2,8,1024]{4,3,2,1,0:T(8,128)(2,1)}, bf16[192,2048]{1,0:T(8,128)(2,1)}, s32[8,192]{1,0:T(8,128)}) custom-call(bf16[192,2048]{1,0:T(8,128)(2,1)} %refs_0_.1, f32[1,2048]{1,0:T(1,128)} %bitcast.30, s32[2,192]{1,0:T(2,128)} %bitcast.31), custom_call_target="tpu_custom_call" | custom-call | flops 402653184 | bytes 4194304 | tf_op jit(solution)/shard_map/dispatch_rows/pallas_call | solution.py:113
  4.1 41.6 %all_to_all.10 = bf16[128,8,1024]{2,1,0:T(8,128)(2,1)S(1)} all-to-all(bf16[128,8,1024]{2,1,0:T(8,128)(2,1)} %bitcast.20), channel_id=1, replica_groups=mesh['ep_0'=4,'ep_1'=4,'tp'=8] {'ep_0','ep_1','tp'}, dimensions={0} | all-to-all | bytes 4194304 | tf_op jit(solution)/shard_map/all_to_all | solution.py:581
  45.7 10.5 %expert_products.1 = bf16[64,2,8,1024]{3,2,1,0:T(8,128)(2,1)} custom-call(bf16[64,2,8,1024]{3,2,1,0:T(8,128)(2,1)S(1)} %bitcast.17, bf16[1,2048,1024]{2,1,0:T(8,128)(2,1)} %refs_1_.2, bf16[1,2048,1024]{2,1,0:T(8,128)(2,1)} %refs_2_.1, bf16[1,1024,2048]{2,1,0:T(8,128)(2,1)} %refs_3_.1), custom_call_target="tpu_custom_call" | custom-call | flops 6442450944 | bytes 12582912 | tf_op jit(solution)/shard_map/expert_products/pallas_call | solution.py:210
  56.2 4.8 %all-to-all-start.1 = ((bf16[128,8,1024]{2,1,0:T(8,128)(2,1)}), bf16[128,8,1024]{2,1,0:T(8,128)(2,1)S(1)}, u32[]{:S(2)}, u32[]{:S(2)}) async-start(bf16[128,8,1024]{2,1,0:T(8,128)(2,1)} %bitcast.19), calls=%async_computation.1 | async-start | bytes 4194304 | tf_op jit(solution)/shard_map/all_to_all | solution.py:581
  61.6 1.8 %device_state.1.refs_0_.refs_10_ = f32[72,128]{1,0:T(8,128)S(1)} custom-call(bf16[64,2048]{1,0:T(8,128)(2,1)} %bitcast.21, bf16[2048,128]{1,0:T(8,128)(2,1)} %refs_4_.2, f32[16,128]{1,0:T(8,128)} %bitcast.23, f32[16,128]{1,0:T(8,128)} %bitcast.25, f32[16,128]{1,0:T(8,128)} %bitcast.27, f32[1]{0:T(128)S(6)} %copy.22.bias_ref.refs_1_), custom_call_target="tpu_custom_call" | custom-call | flops 134217728 | bytes 1048576 | tf_op jit(solution)/shard_map/device_state/pallas_call | solution.py:353
  63.4 2.6 %collective-permute-start.2 = (f32[72,128]{1,0:T(8,128)S(1)}, f32[72,128]{1,0:T(8,128)S(1)}, u32[]{:S(2)}, u32[]{:S(2)}) collective-permute-start(f32[72,128]{1,0:T(8,128)S(1)} %device_state.1.refs_0_.refs_10_), channel_id=1, source_target_pairs={{0,24},{8,0},{16,8},{24,16},{1,25},{9,1},{17,9},{25,17},{2,26},{10... | collective-permute-start | bytes 110600 | tf_op jit(solution)/shard_map/ppermute | solution.py:587
  66.1 0.5 collective-permute-start.1
  66.6 0.6 collective-permute-start
  67.2 0.1 pad_add_fusion.place_ref.refs_0_
  67.3 18.3 %collective-permute-done.2.refs_3_.refs_13_ = f32[72,128]{1,0:T(8,128)S(1)} collective-permute-done((f32[72,128]{1,0:T(8,128)S(1)}, f32[72,128]{1,0:T(8,128)S(1)}, u32[]{:S(2)}, u32[]{:S(2)}) %collective-permute-start.2) | collective-permute-done | bytes 36896 | tf_op jit(solution)/shard_map/ppermute | solution.py:587
  85.6 1.5 %collective-permute-done.1.refs_2_.refs_12_ = f32[72,128]{1,0:T(8,128)S(1)} collective-permute-done((f32[72,128]{1,0:T(8,128)S(1)}, f32[72,128]{1,0:T(8,128)S(1)}, u32[]{:S(2)}, u32[]{:S(2)}) %collective-permute-start.1) | collective-permute-done | bytes 36896 | tf_op jit(solution)/shard_map/ppermute | solution.py:587
  87.1 0.3 collective-permute-done.refs_1_.refs_11_
  87.4 0.8 row_state.1
  88.2 3.3 %collective-permute-start.5 = (f32[72,128]{1,0:T(8,128)S(1)}, f32[72,128]{1,0:T(8,128)S(1)}, u32[]{:S(2)}, u32[]{:S(2)}) collective-permute-start(f32[72,128]{1,0:T(8,128)S(1)} %row_state.1), channel_id=1, source_target_pairs={{0,96},{32,0},{64,32},{96,64},{1,97},{33,1},{65,33},{97,65},{2,98}... | collective-permute-start | bytes 110600 | tf_op jit(solution)/shard_map/ppermute | solution.py:587
  91.4 0.1 collective-permute-start.4
  91.6 0.8 collective-permute-start.3
  92.3 0.2 collective-permute-done.5.refs_16_
  92.5 3.3 %collective-permute-done.4.refs_15_ = f32[72,128]{1,0:T(8,128)S(1)} collective-permute-done((f32[72,128]{1,0:T(8,128)S(1)}, f32[72,128]{1,0:T(8,128)S(1)}, u32[]{:S(2)}, u32[]{:S(2)}) %collective-permute-start.4) | collective-permute-done | bytes 36896 | tf_op jit(solution)/shard_map/ppermute | solution.py:587
  95.9 0.1 collective-permute-done.3.refs_14_
  96.0 7.6 %mixer_rows.1 = (bf16[272,128]{1,0:T(8,128)(2,1)S(1)}, bf16[272,128]{1,0:T(8,128)(2,1)S(1)}, bf16[272,128]{1,0:T(8,128)(2,1)S(1)}, bf16[272,128]{1,0:T(8,128)(2,...) custom-call(s32[3]{0:T(128)S(1)} %pad_add_fusion.place_ref.refs_0_, ...), custom_call_target="tpu_custom_call" | custom-call | flops 1073741824 | bytes 2097152 | tf_op jit(solution)/shard_map/mixer_rows/pallas_call | solution.py:512
  103.6 3.9 %collective-permute-start.6 = (bf16[272,128]{1,0:T(8,128)(2,1)S(1)}, bf16[272,128]{1,0:T(8,128)(2,1)S(1)}, u32[]{:S(2)}, u32[]{:S(2)}) collective-permute-start(bf16[272,128]{1,0:T(8,128)(2,1)S(1)} %get-tuple-element.16), channel_id=1, source_target_pairs={{0,1},{1,2},{2,3},{3,4},{4,5},{5,6},{6,7},{7,0},{8,9},{9,10},{10,1... | collective-permute-start | bytes 208904 | tf_op jit(solution)/shard_map/ppermute | solution.py:587
  107.5 1.2 collective-permute-start.7
  108.8 5.2 %shared_expert.1.refs_3_ = f32[192,2048]{1,0:T(8,128)} custom-call(bf16[192,2048]{1,0:T(8,128)(2,1)} %get-tuple-element.25.n_ref, bf16[2048,384]{1,0:T(8,128)(2,1)} %g_ref.1, bf16[2048,384]{1,0:T(8,128)(2,1)} %u_ref.1, bf16[384,2048]{1,0:T(8,128)(2,1)} %d_ref.1), custom_call_target="tpu_custom_call" | custom-call | flops 905969664 | bytes 4718592 | tf_op jit(solution)/shard_map/shared_expert/pallas_call | solution.py:242
  114.0 1.6 %collective-permute-start.8 = (bf16[272,128]{1,0:T(8,128)(2,1)S(1)}, bf16[272,128]{1,0:T(8,128)(2,1)S(1)}, u32[]{:S(2)}, u32[]{:S(2)}) collective-permute-start(bf16[272,128]{1,0:T(8,128)(2,1)S(1)} %get-tuple-element.18), channel_id=1, source_target_pairs={{0,3},{1,4},{2,5},{3,6},{4,7},{5,0},{6,1},{7,2},{8,11},{9,12},{10,... | collective-permute-start | bytes 208904 | tf_op jit(solution)/shard_map/ppermute | solution.py:587
  115.7 0.4 collective-permute-start.9
  116.1 1.9 %collective-permute-start.10 = (bf16[272,128]{1,0:T(8,128)(2,1)S(1)}, bf16[272,128]{1,0:T(8,128)(2,1)S(1)}, u32[]{:S(2)}, u32[]{:S(2)}) collective-permute-start(bf16[272,128]{1,0:T(8,128)(2,1)S(1)} %get-tuple-element.20), channel_id=1, source_target_pairs={{0,5},{1,6},{2,7},{3,0},{4,1},{5,2},{6,3},{7,4},{8,13},{9,14},{10,... | collective-permute-start | bytes 208904 | tf_op jit(solution)/shard_map/ppermute | solution.py:587
  118.0 0.0 collective-permute-done.6.refs_2_
  118.0 0.8 collective-permute-start.11
  118.8 0.0 collective-permute-done.7.refs_3_
  118.8 1.6 %collective-permute-start.12 = (bf16[272,128]{1,0:T(8,128)(2,1)S(1)}, bf16[272,128]{1,0:T(8,128)(2,1)S(1)}, u32[]{:S(2)}, u32[]{:S(2)}) collective-permute-start(bf16[272,128]{1,0:T(8,128)(2,1)S(1)} %get-tuple-element.22), channel_id=1, source_target_pairs={{0,7},{1,0},{2,1},{3,2},{4,3},{5,4},{6,5},{7,6},{8,15},{9,8},{10,9... | collective-permute-start | bytes 208904 | tf_op jit(solution)/shard_map/ppermute | solution.py:587
  120.4 3.2 %combine.1 = (bf16[192,2048]{1,0:T(8,128)(2,1)}, bf16[1024,2048]{1,0:T(8,128)(2,1)S(1)}) custom-call(bf16[1024,1024]{1,0:T(8,128)(2,1)S(1)} %bitcast.16, s32[8,192]{1,0:T(8,128)S(1)} %copy-done, f32[2,192]{1,0:T(2,128)S(1)} %bitcast.18, f32[192,2048]{1,0:T(8,128)} %shared_expert.1.refs_3_, bf16[1024,2048]{1,0:T(8,128)(2,1)} %refs_4_.3), custom_call_target="tpu_custom_call" | custom-call | flops 1610612736 | bytes 2097152 | tf_op jit(solution)/shard_map/combine/pallas_call | solution.py:291
  123.7 2.6 %project.1 = bf16[256,2048]{1,0:T(8,128)(2,1)} custom-call(s32[3]{0:T(128)S(1)} %pad_add_fusion.place_ref.refs_0_, bf16[272,128]{1,0:T(8,128)(2,1)S(1)} %get-tuple-element.15.refs_1_, bf16[272,128]{1,0:T(8,128)(2,1)S(1)} %collective-permute-done.6.refs_2_, bf16[272,128]{1,0:T(8,128)(2,1)S(1)} %collective-permute-done.7.refs_3_, ...), custom_call_target="tpu_custom_call" | custom-call | flops 1073741824 | bytes 4194304 | tf_op jit(solution)/shard_map/project/pallas_call | solution.py:564
  (10 shorter events, 0.0 us)
Async XLA Ops:
  56.2 64.2 %all-to-all-start.1 = ((bf16[128,8,1024]{2,1,0:T(8,128)(2,1)}), bf16[128,8,1024]{2,1,0:T(8,128)(2,1)S(1)}, u32[]{:S(2)}, u32[]{:S(2)}) async-start(bf16[128,8,1024]{2,1,0:T(8,128)(2,1)} %bitcast.19), calls=%async_computation.1 | async-start | bytes 4194304 | tf_op jit(solution)/shard_map/all_to_all | solution.py:581
  63.4 22.1 %collective-permute-start.2 = (f32[72,128]{1,0:T(8,128)S(1)}, f32[72,128]{1,0:T(8,128)S(1)}, u32[]{:S(2)}, u32[]{:S(2)}) collective-permute-start(f32[72,128]{1,0:T(8,128)S(1)} %device_state.1.refs_0_.refs_10_), channel_id=1, source_target_pairs={{0,24},{8,0},{16,8},{24,16},{1,25},{9,1},{17,9},{25,17},{2,26},{10... | collective-permute-start | bytes 110600 | tf_op jit(solution)/shard_map/ppermute | solution.py:587
  66.1 21.0 %collective-permute-start.1 = (f32[72,128]{1,0:T(8,128)S(1)}, f32[72,128]{1,0:T(8,128)S(1)}, u32[]{:S(2)}, u32[]{:S(2)}) collective-permute-start(f32[72,128]{1,0:T(8,128)S(1)} %device_state.1.refs_0_.refs_10_), channel_id=1, source_target_pairs={{0,16},{8,24},{16,0},{24,8},{1,17},{9,25},{17,1},{25,9},{2,18},{10... | collective-permute-start | bytes 110600 | tf_op jit(solution)/shard_map/ppermute | solution.py:587
  66.6 20.8 %collective-permute-start = (f32[72,128]{1,0:T(8,128)S(1)}, f32[72,128]{1,0:T(8,128)S(1)}, u32[]{:S(2)}, u32[]{:S(2)}) collective-permute-start(f32[72,128]{1,0:T(8,128)S(1)} %device_state.1.refs_0_.refs_10_), channel_id=1, source_target_pairs={{0,8},{8,16},{16,24},{24,0},{1,9},{9,17},{17,25},{25,1},{2,10},{10... | collective-permute-start | bytes 110600 | tf_op jit(solution)/shard_map/ppermute | solution.py:587
  88.2 4.3 %collective-permute-start.5 = (f32[72,128]{1,0:T(8,128)S(1)}, f32[72,128]{1,0:T(8,128)S(1)}, u32[]{:S(2)}, u32[]{:S(2)}) collective-permute-start(f32[72,128]{1,0:T(8,128)S(1)} %row_state.1), channel_id=1, source_target_pairs={{0,96},{32,0},{64,32},{96,64},{1,97},{33,1},{65,33},{97,65},{2,98}... | collective-permute-start | bytes 110600 | tf_op jit(solution)/shard_map/ppermute | solution.py:587
  91.4 4.4 %collective-permute-start.4 = (f32[72,128]{1,0:T(8,128)S(1)}, f32[72,128]{1,0:T(8,128)S(1)}, u32[]{:S(2)}, u32[]{:S(2)}) collective-permute-start(f32[72,128]{1,0:T(8,128)S(1)} %row_state.1), channel_id=1, source_target_pairs={{0,64},{32,96},{64,0},{96,32},{1,65},{33,97},{65,1},{97,33},{2,66}... | collective-permute-start | bytes 110600 | tf_op jit(solution)/shard_map/ppermute | solution.py:587
  91.6 4.4 %collective-permute-start.3 = (f32[72,128]{1,0:T(8,128)S(1)}, f32[72,128]{1,0:T(8,128)S(1)}, u32[]{:S(2)}, u32[]{:S(2)}) collective-permute-start(f32[72,128]{1,0:T(8,128)S(1)} %row_state.1), channel_id=1, source_target_pairs={{0,32},{32,64},{64,96},{96,0},{1,33},{33,65},{65,97},{97,1},{2,34}... | collective-permute-start | bytes 110600 | tf_op jit(solution)/shard_map/ppermute | solution.py:587
  103.6 14.4 %collective-permute-start.6 = (bf16[272,128]{1,0:T(8,128)(2,1)S(1)}, bf16[272,128]{1,0:T(8,128)(2,1)S(1)}, u32[]{:S(2)}, u32[]{:S(2)}) collective-permute-start(bf16[272,128]{1,0:T(8,128)(2,1)S(1)} %get-tuple-element.16), channel_id=1, source_target_pairs={{0,1},{1,2},{2,3},{3,4},{4,5},{5,6},{6,7},{7,0},{8,9},{9,10},{10,1... | collective-permute-start | bytes 208904 | tf_op jit(solution)/shard_map/ppermute | solution.py:587
  107.5 11.3 %collective-permute-start.7 = (bf16[272,128]{1,0:T(8,128)(2,1)S(1)}, bf16[272,128]{1,0:T(8,128)(2,1)S(1)}, u32[]{:S(2)}, u32[]{:S(2)}) collective-permute-start(bf16[272,128]{1,0:T(8,128)(2,1)S(1)} %get-tuple-element.17), channel_id=1, source_target_pairs={{0,2},{1,3},{2,4},{3,5},{4,6},{5,7},{6,0},{7,1},{8,10},{9,11},{10,... | collective-permute-start | bytes 208904 | tf_op jit(solution)/shard_map/ppermute | solution.py:587
  108.8 11.7 %copy-start = (s32[8,192]{1,0:T(8,128)S(1)}, s32[8,192]{1,0:T(8,128)}, u32[]{:S(2)}) copy-start(s32[8,192]{1,0:T(8,128)} %get-tuple-element.24.refs_1_) | copy-start | bytes 18436
  108.8 11.7 %copy-start.1 = (f32[192,2]{0,1:T(2,128)S(1)}, f32[192,2]{0,1:T(2,128)}, u32[]{:S(2)}) copy-start(f32[192,2]{0,1:T(2,128)} %param.33) | copy-start | bytes 4612
  114.0 9.7 %collective-permute-start.8 = (bf16[272,128]{1,0:T(8,128)(2,1)S(1)}, bf16[272,128]{1,0:T(8,128)(2,1)S(1)}, u32[]{:S(2)}, u32[]{:S(2)}) collective-permute-start(bf16[272,128]{1,0:T(8,128)(2,1)S(1)} %get-tuple-element.18), channel_id=1, source_target_pairs={{0,3},{1,4},{2,5},{3,6},{4,7},{5,0},{6,1},{7,2},{8,11},{9,12},{10,... | collective-permute-start | bytes 208904 | tf_op jit(solution)/shard_map/ppermute | solution.py:587
  115.7 8.0 %collective-permute-start.9 = (bf16[272,128]{1,0:T(8,128)(2,1)S(1)}, bf16[272,128]{1,0:T(8,128)(2,1)S(1)}, u32[]{:S(2)}, u32[]{:S(2)}) collective-permute-start(bf16[272,128]{1,0:T(8,128)(2,1)S(1)} %get-tuple-element.19), channel_id=1, source_target_pairs={{0,4},{1,5},{2,6},{3,7},{4,0},{5,1},{6,2},{7,3},{8,12},{9,13},{10,... | collective-permute-start | bytes 208904 | tf_op jit(solution)/shard_map/ppermute | solution.py:587
  116.1 7.6 %collective-permute-start.10 = (bf16[272,128]{1,0:T(8,128)(2,1)S(1)}, bf16[272,128]{1,0:T(8,128)(2,1)S(1)}, u32[]{:S(2)}, u32[]{:S(2)}) collective-permute-start(bf16[272,128]{1,0:T(8,128)(2,1)S(1)} %get-tuple-element.20), channel_id=1, source_target_pairs={{0,5},{1,6},{2,7},{3,0},{4,1},{5,2},{6,3},{7,4},{8,13},{9,14},{10,... | collective-permute-start | bytes 208904 | tf_op jit(solution)/shard_map/ppermute | solution.py:587
  118.0 5.7 %collective-permute-start.11 = (bf16[272,128]{1,0:T(8,128)(2,1)S(1)}, bf16[272,128]{1,0:T(8,128)(2,1)S(1)}, u32[]{:S(2)}, u32[]{:S(2)}) collective-permute-start(bf16[272,128]{1,0:T(8,128)(2,1)S(1)} %get-tuple-element.21), channel_id=1, source_target_pairs={{0,6},{1,7},{2,0},{3,1},{4,2},{5,3},{6,4},{7,5},{8,14},{9,15},{10,... | collective-permute-start | bytes 208904 | tf_op jit(solution)/shard_map/ppermute | solution.py:587
  118.8 4.9 %collective-permute-start.12 = (bf16[272,128]{1,0:T(8,128)(2,1)S(1)}, bf16[272,128]{1,0:T(8,128)(2,1)S(1)}, u32[]{:S(2)}, u32[]{:S(2)}) collective-permute-start(bf16[272,128]{1,0:T(8,128)(2,1)S(1)} %get-tuple-element.22), channel_id=1, source_target_pairs={{0,7},{1,0},{2,1},{3,2},{4,3},{5,4},{6,5},{7,6},{8,15},{9,8},{10,9... | collective-permute-start | bytes 208904 | tf_op jit(solution)/shard_map/ppermute | solution.py:587

commit v3 on v2

--- a/solution.py
+++ b/solution.py
@@ -61,31 +61,36 @@
     return [idx[j : j + 1, :] * cap + places[j].astype(jnp.int32) for j in range(2)]
 
 
-def dispatch_body(
-    cap, x_hbm, gain_hbm, idx_hbm, send_hbm, normed_hbm, slots_hbm,
-    x_ref, gain_ref, idx_ref, send_ref, normed_ref, slots_ref, in_sems, out_sems,
-):
+def start_body(cap, *refs):
+    bias_ref = refs[0]
+    sources = refs[1:9]
+    send_hbm, normed_hbm, slots_hbm, state_ref = refs[9:13]
+    (idx_ref, gain_ref, in_ref, forget_ref, extra_ref, k_ref, v_ref, x_ref,
+     send_ref, normed_ref, slots_ref, in_sems, out_sems) = refs[13:]
     tokens, width = x_ref.shape
     half = width // 2
     pieces, pairs = send_ref.shape[0:2]
     experts = 2 * pieces * pairs
+    kept = (idx_ref, gain_ref, in_ref, forget_ref, extra_ref, k_ref, v_ref, x_ref)
     loads = [
         pltpu.make_async_copy(src, dst, in_sems.at[i])
-        for i, (src, dst) in enumerate(((idx_hbm, idx_ref), (gain_hbm, gain_ref), (x_hbm, x_ref)))
+        for i, (src, dst) in enumerate(zip(sources, kept))
     ]
     for load in loads:
         load.start()
-    loads[0].wait()
+    for load in loads[:-1]:
+        load.wait()
     slot0, slot1 = copy_slots(idx_ref[...], cap, experts)
     slots_ref[...] = jnp.concatenate([slot0, slot1] * 4, axis=0)
     stores = [pltpu.make_async_copy(slots_ref, slots_hbm, out_sems.at[pieces])]
     stores[0].start()
-    loads[1].wait()
-    loads[2].wait()
+    write_state(k_ref, v_ref, in_ref, forget_ref, extra_ref, bias_ref, state_ref)
+    loads[-1].wait()
     x = x_ref[...].astype(F32)
     scale = lax.rsqrt(jnp.mean(x * x, axis=-1, keepdims=True) + 1e-06)
     normed = (x * scale * gain_ref[...]).astype(BF16)
     normed_ref[...] = normed
+    stores.append(pltpu.make_async_copy(normed_ref, normed_hbm, out_sems.at[pieces + 1]))
     lower = iota((pairs, 8, half), 1) < 4
     rows = pairs * 2 * cap
     for p in range(pieces):
@@ -98,41 +103,41 @@
         send_ref[p, :, 1] = odd.astype(BF16)
         stores.append(pltpu.make_async_copy(send_ref.at[p], send_hbm.at[p], out_sems.at[p]))
         stores[-1].start()
-    stores.append(pltpu.make_async_copy(normed_ref, normed_hbm, out_sems.at[pieces + 1]))
-    stores[-1].start()
+        if p == 0:
+            stores[1].start()
     for store in stores:
         store.wait()
 
 
-def dispatch_rows(x, gain, idx, cap, experts):
+def start(x, gain, idx, keys, values, in_gate, forget, extra, bias, cap, experts):
     tokens, width = x.shape
     pieces = 4
     shape = (pieces, experts // (2 * pieces), 2, 2 * cap, width // 2)
+    inputs = (idx, gain, in_gate, forget, extra, keys, values, x)
     hbm = pl.BlockSpec(memory_space=pltpu.HBM)
-    body = lambda *refs: dispatch_body(cap, *refs)
+    body = lambda *refs: start_body(cap, *refs)
     return pl.pallas_call(
         body,
-        in_specs=[hbm] * 3,
-        out_specs=[hbm] * 3,
+        in_specs=[pl.BlockSpec(memory_space=pltpu.SMEM)] + [hbm] * len(inputs),
+        out_specs=[hbm] * 3 + [pl.BlockSpec(memory_space=pltpu.VMEM)],
         out_shape=[
             pltpu.HBM(shape, BF16),
             pltpu.HBM((tokens, width), BF16),
             pltpu.HBM((8, tokens), jnp.int32),
+            jax.ShapeDtypeStruct((keys.shape[0] + 8, BLK), F32),
         ],
-        scratch_shapes=[
-            pltpu.VMEM((tokens, width), BF16),
-            pltpu.VMEM((1, width), F32),
-            pltpu.VMEM((2, tokens), jnp.int32),
+        scratch_shapes=[pltpu.VMEM(a.shape, a.dtype) for a in inputs]
+        + [
             pltpu.VMEM(shape, BF16),
             pltpu.VMEM((tokens, width), BF16),
             pltpu.VMEM((8, tokens), jnp.int32),
-            pltpu.SemaphoreType.DMA((3,)),
+            pltpu.SemaphoreType.DMA((len(inputs),)),
             pltpu.SemaphoreType.DMA((pieces + 2,)),
         ],
-        compiler_params=params(20),
+        compiler_params=params(24),
         cost_estimate=cost(2 * experts * cap * tokens * width, 4 * experts * cap * width),
-        name="dispatch_rows",
-    )(*in_hbm(x, gain, idx))
+        name="start",
+    )(bias, *in_hbm(*inputs))
 
 
 def swap_halves(even, odd, lower):
@@ -177,24 +182,38 @@
         x_ref[at, 0:half] = first.reshape(group * 8, half).astype(BF16)
         x_ref[at, half:] = last.reshape(group * 8, half).astype(BF16)
 
+    lower = iota((pairs, 8, part), 1) < 4
+
+    def activate(p, gate, up):
+        h_ref[:, p * wide : (p + 1) * wide] = (gate * jax.nn.sigmoid(gate) * up).astype(BF16)
+
+    def leave(p, first, last):
+        even, odd = swap_halves(first.reshape(pairs, 8, part), last.reshape(pairs, 8, part), lower)
+        o_ref[p, :, 0] = even.astype(BF16)
+        o_ref[p, :, 1] = odd.astype(BF16)
+        stores[p].start()
+
+    ahead = None
     for p in range(pieces):
         for copy in first_loads[p]:
             copy.wait()
         x = x_ref[...]
-        gate = dot(x, g_ref[p])
-        up = dot(x, u_ref[p])
-        h_ref[:, p * wide : (p + 1) * wide] = (gate * jax.nn.sigmoid(gate) * up).astype(BF16)
-    lower = iota((pairs, 8, part), 1) < 4
+        products = (dot(x, g_ref[p]), dot(x, u_ref[p]))
+        if ahead is not None:
+            activate(p - 1, *ahead)
+        ahead = products
+    activate(pieces - 1, *ahead)
+    ahead = None
+    for copies in last_loads:
+        for copy in copies:
+            copy.wait()
     for p in range(pieces):
-        for copy in last_loads[p]:
-            copy.wait()
         h = h_ref[...]
-        first = dot(h, d_ref[p, 0]).reshape(pairs, 8, part)
-        last = dot(h, d_ref[p, 1]).reshape(pairs, 8, part)
-        even, odd = swap_halves(first, last, lower)
-        o_ref[p, :, 0] = even.astype(BF16)
-        o_ref[p, :, 1] = odd.astype(BF16)
-        stores[p].start()
+        products = (dot(h, d_ref[p, 0]), dot(h, d_ref[p, 1]))
+        if ahead is not None:
+            leave(p - 1, *ahead)
+        ahead = products
+    leave(pieces - 1, *ahead)
     for store in stores:
         store.wait()
 
@@ -308,8 +327,8 @@
     )(back, slots, weights, *in_hbm(shared, mixer_weight))
 
 
-def gate_rows(in_ref, forget_ref, extra_ref, bias_ref):
-    x = forget_ref[...] + bias_ref[0]
+def gate_rows(in_ref, forget_ref, extra_ref, bias):
+    x = forget_ref[...] + bias
     log_forget = jnp.minimum(x, 0.0) - jnp.log1p(jnp.exp(-jnp.abs(x))) + extra_ref[...]
     upper = jnp.where(iota((BLK, BLK), 0) <= iota((BLK, BLK), 1), 1.0, 0.0)
     cumulative = exact_dot(log_forget, upper)
@@ -318,10 +337,10 @@
     return in_ref[...], cumulative, total
 
 
-def state_body(k_ref, v_ref, in_ref, forget_ref, extra_ref, bias_ref, out_ref):
+def write_state(k_ref, v_ref, in_ref, forget_ref, extra_ref, bias_ref, out_ref):
     key_dim, length = k_ref.shape
     blocks = length // BLK
-    in_gate, cumulative, total = gate_rows(in_ref, forget_ref, extra_ref, bias_ref)
+    in_gate, cumulative, total = gate_rows(in_ref, forget_ref, extra_ref, bias_ref[0])
     sums = [jnp.zeros((1, BLK), F32)]
     for j in reversed(range(1, blocks)):
         sums.insert(0, sums[0] + total[j : j + 1, :])
@@ -348,18 +367,6 @@
     out_ref[key_dim:, :] = tail
 
 
-def device_state(keys, values, in_gate, forget, extra, bias):
-    key_dim, length = keys.shape
-    return pl.pallas_call(
-        state_body,
-        in_specs=[pl.BlockSpec(memory_space=pltpu.VMEM)] * 5 + [pl.BlockSpec(memory_space=pltpu.SMEM)],
-        out_shape=jax.ShapeDtypeStruct((key_dim + 8, BLK), F32),
-        compiler_params=params(8),
-        cost_estimate=cost(8 * length * key_dim * BLK, 4 * length * BLK),
-        name="device_state",
-    )(*in_hbm(keys, values, in_gate, forget, extra), bias)
-
-
 def merge_states(refs, keys, counted, key_dim):
     tails = [ref[key_dim : key_dim + 1, :] for ref in refs]
     tops = [t[:, key_dim : key_dim + 1] for t in tails]
@@ -451,7 +458,7 @@
     peers = len(outs)
     tokens = length // peers
     per_chunk = tokens // BLK
-    in_gate, cumulative, total = gate_rows(in_ref, forget_ref, extra_ref, bias_ref)
+    in_gate, cumulative, total = gate_rows(in_ref, forget_ref, extra_ref, bias_ref[0])
     state, top = incoming_state(place_ref, rows, columns, key_dim)
     gap = total - cumulative + in_gate
     block_top = jnp.max(gap, axis=1, keepdims=True)
@@ -615,10 +622,6 @@
     ep_count, tp_count = lax.axis_size(EP), lax.axis_size("tp")
     experts = ep_count * tp_count
     cap = 4
-    send, normed, slots = dispatch_rows(
-        second_batch_input, expert_norm_gain[None, :], routed_expert_index.T, cap, experts
-    )
-    landed = exchange(send.reshape(experts, 2 * cap, -1), EP_TP)
 
     def by_block(a):
         return a.reshape(length // BLK, BLK)
@@ -629,11 +632,24 @@
         by_block(extra_log_forget),
     )
     query_rows, key_rows = queries.T, head_key_rows.T
+    send, normed, slots, own = start(
+        second_batch_input,
+        expert_norm_gain[None, :],
+        routed_expert_index.T,
+        key_rows,
+        head_value_rows,
+        in_gate,
+        forget,
+        extra,
+        head_forget_bias,
+        cap,
+        experts,
+    )
     place = jnp.stack([lax.axis_index(a).astype(jnp.int32) for a in ("ep_0", "ep_1", "tp")])
-    own = device_state(key_rows, head_value_rows, in_gate, forget, extra, head_forget_bias)
     row_states = [own] + from_earlier([own] * (lax.axis_size("ep_1") - 1), "ep_1")
     row_total = row_state(place, row_states)
     column_states = from_earlier([row_total] * (lax.axis_size("ep_0") - 1), "ep_0")
+    landed = exchange(send.reshape(experts, 2 * cap, -1), EP_TP)
     chunks = mixer_rows(
         place,
         head_forget_bias,

time: 127 us -> 128 us (level)
  waiting for transfers between devices: 23.8 us -> 26.2 us
    ppermute x13, waiting for transfers between devices: 23.8 us -> 26.2 us  [from_earlier(): lax.ppermute(shard, axis, [(p, (p + k) % count) for p in range(count)])]
    pallas_call x2 -> x1, Pallas kernels: 5.3 us -> 4.6 us  [start(): pl.pallas_call(body, in_specs=[pl.BlockSpec(memory_space=pltpu.SMEM)] + [...]
  transfers between devices with their start and end apart: 14 -> 14, of which waited for: 6 -> 6; matrix products, arithmetic and copies ran while one was open for 0% -> 0% of each run, Pallas kernels for 15% -> 13%
where the time goes in v3:
time: 128 us
  blocking collectives  41.6 us (32%)
  Pallas kernels  34.1 us (27%)
  waiting for transfers between devices  26.2 us (20%)
  starting transfers between devices  24.3 us (19%)
  between operations  1.54 us (1%)
    all_to_all x1, blocking collectives, exchange(): return lax.all_to_all(x, axes, split_axis=0, concat_axis=0, tiled=True)  41.6 us
    ppermute x13, waiting for transfers between devices, from_earlier(): lax.ppermute(shard, axis, [(p, (p + k) % count) for p in range(count)])  26.2 us
    ppermute x13, starting transfers between devices, from_earlier(): lax.ppermute(shard, axis, [(p, (p + k) % count) for p in range(count)])  19.6 us
    pallas_call x1, Pallas kernels, expert_products(): pl.pallas_call(body, in_specs=[pl.BlockSpec(memory_space=pltpu.VMEM), hbm...  10.1 us
    pallas_call x1, Pallas kernels, mixer_rows(): pl.pallas_call(body, in_specs=[smem, smem] + [vmem] * (8 + len(rows) + le...  7.59 us
    pallas_call x1, Pallas kernels, shared_expert(): pl.pallas_call(shared_body, out_shape=pltpu.HBM((tokens, width), F32), co...  5.24 us
    all_to_all x1, starting transfers between devices, exchange(): return lax.all_to_all(x, axes, split_axis=0, concat_axis=0, tiled=True)  4.76 us
    pallas_call x1, Pallas kernels, start(): pl.pallas_call(body, in_specs=[pl.BlockSpec(memory_space=pltpu.SMEM)] + [...  4.6 us
  transfers between devices with their start and end apart: 14, of which 6 were waited for; matrix products, arithmetic and copies ran while one was open for 0% of the time, Pallas kernels for 13%

profile of v3, /device:TPU:1, one launch (start us, length us, event | category | flops | bytes accessed | tf_op | source)
XLA Modules:
  0.0 127.8 jit_solution(13107837046404874232)
XLA Ops:
  1.3 4.6 %start.1 = (bf16[4,16,2,8,1024]{4,3,2,1,0:T(8,128)(2,1)}, bf16[192,2048]{1,0:T(8,128)(2,1)}, s32[8,192]{1,0:T(8,128)}, f32[72,128]{1,0:T(8,128)S(1)}) custom-call(f32[1]{0:T(128)S(6)} %copy.22.refs_0_.refs_1_, s32[2,192]{1,0:T(2,128)} %bitcast.30, f32[1,2048]{1,0:T(1,128)} %bitcast.23, f32[16,128]{1,0:T(8,128)} %bitcast.24, f32[16,128]{1,0:T(8,128)} %bitcast.26, ...), custom_call_target="tpu_custom_call" | custom-call | flops 402653184 | bytes 4194304 | tf_op jit(solution)/shard_map/start/pallas_call | solution.py:119
  5.9 41.6 %all_to_all.10 = bf16[128,8,1024]{2,1,0:T(8,128)(2,1)S(1)} all-to-all(bf16[128,8,1024]{2,1,0:T(8,128)(2,1)} %bitcast.20), channel_id=1, replica_groups=mesh['ep_0'=4,'ep_1'=4,'tp'=8] {'ep_0','ep_1','tp'}, dimensions={0} | all-to-all | bytes 4194304 | tf_op jit(solution)/shard_map/all_to_all | solution.py:588
  47.5 10.1 %expert_products.1 = bf16[64,2,8,1024]{3,2,1,0:T(8,128)(2,1)} custom-call(bf16[64,2,8,1024]{3,2,1,0:T(8,128)(2,1)S(1)} %bitcast.17, bf16[1,2048,1024]{2,1,0:T(8,128)(2,1)} %refs_1_.2, bf16[1,2048,1024]{2,1,0:T(8,128)(2,1)} %refs_2_.1, bf16[1,1024,2048]{2,1,0:T(8,128)(2,1)} %refs_3_.1), custom_call_target="tpu_custom_call" | custom-call | flops 6442450944 | bytes 12582912 | tf_op jit(solution)/shard_map/expert_products/pallas_call | solution.py:229
  57.6 4.8 %all-to-all-start.1 = ((bf16[128,8,1024]{2,1,0:T(8,128)(2,1)}), bf16[128,8,1024]{2,1,0:T(8,128)(2,1)S(1)}, u32[]{:S(2)}, u32[]{:S(2)}) async-start(bf16[128,8,1024]{2,1,0:T(8,128)(2,1)} %bitcast.19), calls=%async_computation.1 | async-start | bytes 4194304 | tf_op jit(solution)/shard_map/all_to_all | solution.py:588
  62.3 2.7 %collective-permute-start.2 = (f32[72,128]{1,0:T(8,128)S(1)}, f32[72,128]{1,0:T(8,128)S(1)}, u32[]{:S(2)}, u32[]{:S(2)}) collective-permute-start(f32[72,128]{1,0:T(8,128)S(1)} %get-tuple-element.16.refs_0_.refs_10_), channel_id=1, source_target_pairs={{0,24},{8,0},{16,8},{24,16},{1,25},{9,1},{17,9},{25,17},{2,26},{10... | collective-permute-start | bytes 110600 | tf_op jit(solution)/shard_map/ppermute | solution.py:594
  65.0 0.5 collective-permute-start.1
  65.6 0.6 collective-permute-start
  66.1 0.1 pad_add_fusion.place_ref.refs_0_
  66.2 20.7 %collective-permute-done.2.refs_3_.refs_13_ = f32[72,128]{1,0:T(8,128)S(1)} collective-permute-done((f32[72,128]{1,0:T(8,128)S(1)}, f32[72,128]{1,0:T(8,128)S(1)}, u32[]{:S(2)}, u32[]{:S(2)}) %collective-permute-start.2) | collective-permute-done | bytes 36896 | tf_op jit(solution)/shard_map/ppermute | solution.py:594
  87.0 1.5 %collective-permute-done.1.refs_2_.refs_12_ = f32[72,128]{1,0:T(8,128)S(1)} collective-permute-done((f32[72,128]{1,0:T(8,128)S(1)}, f32[72,128]{1,0:T(8,128)S(1)}, u32[]{:S(2)}, u32[]{:S(2)}) %collective-permute-start.1) | collective-permute-done | bytes 36896 | tf_op jit(solution)/shard_map/ppermute | solution.py:594
  88.5 0.3 collective-permute-done.refs_1_.refs_11_
  88.8 0.8 row_state.1
  89.5 3.3 %collective-permute-start.5 = (f32[72,128]{1,0:T(8,128)S(1)}, f32[72,128]{1,0:T(8,128)S(1)}, u32[]{:S(2)}, u32[]{:S(2)}) collective-permute-start(f32[72,128]{1,0:T(8,128)S(1)} %row_state.1), channel_id=1, source_target_pairs={{0,96},{32,0},{64,32},{96,64},{1,97},{33,1},{65,33},{97,65},{2,98}... | collective-permute-start | bytes 110600 | tf_op jit(solution)/shard_map/ppermute | solution.py:594
  92.8 0.1 collective-permute-start.4
  92.9 0.8 collective-permute-start.3
  93.7 0.2 collective-permute-done.5.refs_16_
  93.9 3.3 %collective-permute-done.4.refs_15_ = f32[72,128]{1,0:T(8,128)S(1)} collective-permute-done((f32[72,128]{1,0:T(8,128)S(1)}, f32[72,128]{1,0:T(8,128)S(1)}, u32[]{:S(2)}, u32[]{:S(2)}) %collective-permute-start.4) | collective-permute-done | bytes 36896 | tf_op jit(solution)/shard_map/ppermute | solution.py:594
  97.2 0.1 collective-permute-done.3.refs_14_
  97.3 7.6 %mixer_rows.1 = (bf16[272,128]{1,0:T(8,128)(2,1)S(1)}, bf16[272,128]{1,0:T(8,128)(2,1)S(1)}, bf16[272,128]{1,0:T(8,128)(2,1)S(1)}, bf16[272,128]{1,0:T(8,128)(2,...) custom-call(s32[3]{0:T(128)S(1)} %pad_add_fusion.place_ref.refs_0_, ...), custom_call_target="tpu_custom_call" | custom-call | flops 1073741824 | bytes 2097152 | tf_op jit(solution)/shard_map/mixer_rows/pallas_call | solution.py:519
  104.9 3.9 %collective-permute-start.6 = (bf16[272,128]{1,0:T(8,128)(2,1)S(1)}, bf16[272,128]{1,0:T(8,128)(2,1)S(1)}, u32[]{:S(2)}, u32[]{:S(2)}) collective-permute-start(bf16[272,128]{1,0:T(8,128)(2,1)S(1)} %get-tuple-element.18), channel_id=1, source_target_pairs={{0,1},{1,2},{2,3},{3,4},{4,5},{5,6},{6,7},{7,0},{8,9},{9,10},{10,1... | collective-permute-start | bytes 208904 | tf_op jit(solution)/shard_map/ppermute | solution.py:594
  108.9 1.3 collective-permute-start.7
  110.1 5.2 %shared_expert.1.refs_3_ = f32[192,2048]{1,0:T(8,128)} custom-call(bf16[192,2048]{1,0:T(8,128)(2,1)} %get-tuple-element.27.n_ref, bf16[2048,384]{1,0:T(8,128)(2,1)} %g_ref.1, bf16[2048,384]{1,0:T(8,128)(2,1)} %u_ref.1, bf16[384,2048]{1,0:T(8,128)(2,1)} %d_ref.1), custom_call_target="tpu_custom_call" | custom-call | flops 905969664 | bytes 4718592 | tf_op jit(solution)/shard_map/shared_expert/pallas_call | solution.py:261
  115.4 1.6 %collective-permute-start.8 = (bf16[272,128]{1,0:T(8,128)(2,1)S(1)}, bf16[272,128]{1,0:T(8,128)(2,1)S(1)}, u32[]{:S(2)}, u32[]{:S(2)}) collective-permute-start(bf16[272,128]{1,0:T(8,128)(2,1)S(1)} %get-tuple-element.20), channel_id=1, source_target_pairs={{0,3},{1,4},{2,5},{3,6},{4,7},{5,0},{6,1},{7,2},{8,11},{9,12},{10,... | collective-permute-start | bytes 208904 | tf_op jit(solution)/shard_map/ppermute | solution.py:594
  117.0 0.4 collective-permute-start.9
  117.5 1.9 %collective-permute-start.10 = (bf16[272,128]{1,0:T(8,128)(2,1)S(1)}, bf16[272,128]{1,0:T(8,128)(2,1)S(1)}, u32[]{:S(2)}, u32[]{:S(2)}) collective-permute-start(bf16[272,128]{1,0:T(8,128)(2,1)S(1)} %get-tuple-element.22), channel_id=1, source_target_pairs={{0,5},{1,6},{2,7},{3,0},{4,1},{5,2},{6,3},{7,4},{8,13},{9,14},{10,... | collective-permute-start | bytes 208904 | tf_op jit(solution)/shard_map/ppermute | solution.py:594
  119.4 0.0 collective-permute-done.6.refs_2_
  119.4 0.8 collective-permute-start.11
  120.2 1.6 %collective-permute-start.12 = (bf16[272,128]{1,0:T(8,128)(2,1)S(1)}, bf16[272,128]{1,0:T(8,128)(2,1)S(1)}, u32[]{:S(2)}, u32[]{:S(2)}) collective-permute-start(bf16[272,128]{1,0:T(8,128)(2,1)S(1)} %get-tuple-element.24), channel_id=1, source_target_pairs={{0,7},{1,0},{2,1},{3,2},{4,3},{5,4},{6,5},{7,6},{8,15},{9,8},{10,9... | collective-permute-start | bytes 208904 | tf_op jit(solution)/shard_map/ppermute | solution.py:594
  121.8 0.0 all-to-all-done.1
  121.8 3.2 %combine.1 = (bf16[192,2048]{1,0:T(8,128)(2,1)}, bf16[1024,2048]{1,0:T(8,128)(2,1)S(1)}) custom-call(bf16[1024,1024]{1,0:T(8,128)(2,1)S(1)} %bitcast.16, s32[8,192]{1,0:T(8,128)S(1)} %copy-done, f32[2,192]{1,0:T(2,128)S(1)} %bitcast.18, f32[192,2048]{1,0:T(8,128)} %shared_expert.1.refs_3_, bf16[1024,2048]{1,0:T(8,128)(2,1)} %refs_4_.3), custom_call_target="tpu_custom_call" | custom-call | flops 1610612736 | bytes 2097152 | tf_op jit(solution)/shard_map/combine/pallas_call | solution.py:310
  125.1 0.0 collective-permute-done.8.refs_4_
  125.1 2.6 %project.1 = bf16[256,2048]{1,0:T(8,128)(2,1)} custom-call(s32[3]{0:T(128)S(1)} %pad_add_fusion.place_ref.refs_0_, bf16[272,128]{1,0:T(8,128)(2,1)S(1)} %get-tuple-element.17.refs_1_, bf16[272,128]{1,0:T(8,128)(2,1)S(1)} %collective-permute-done.6.refs_2_, bf16[272,128]{1,0:T(8,128)(2,1)S(1)} %collective-permute-done.7.refs_3_, ...), custom_call_target="tpu_custom_call" | custom-call | flops 1073741824 | bytes 4194304 | tf_op jit(solution)/shard_map/project/pallas_call | solution.py:571
  (9 shorter events, 0.0 us)
Async XLA Ops:
  57.6 64.2 %all-to-all-start.1 = ((bf16[128,8,1024]{2,1,0:T(8,128)(2,1)}), bf16[128,8,1024]{2,1,0:T(8,128)(2,1)S(1)}, u32[]{:S(2)}, u32[]{:S(2)}) async-start(bf16[128,8,1024]{2,1,0:T(8,128)(2,1)} %bitcast.19), calls=%async_computation.1 | async-start | bytes 4194304 | tf_op jit(solution)/shard_map/all_to_all | solution.py:588
  62.3 24.6 %collective-permute-start.2 = (f32[72,128]{1,0:T(8,128)S(1)}, f32[72,128]{1,0:T(8,128)S(1)}, u32[]{:S(2)}, u32[]{:S(2)}) collective-permute-start(f32[72,128]{1,0:T(8,128)S(1)} %get-tuple-element.16.refs_0_.refs_10_), channel_id=1, source_target_pairs={{0,24},{8,0},{16,8},{24,16},{1,25},{9,1},{17,9},{25,17},{2,26},{10... | collective-permute-start | bytes 110600 | tf_op jit(solution)/shard_map/ppermute | solution.py:594
  65.0 23.5 %collective-permute-start.1 = (f32[72,128]{1,0:T(8,128)S(1)}, f32[72,128]{1,0:T(8,128)S(1)}, u32[]{:S(2)}, u32[]{:S(2)}) collective-permute-start(f32[72,128]{1,0:T(8,128)S(1)} %get-tuple-element.16.refs_0_.refs_10_), channel_id=1, source_target_pairs={{0,16},{8,24},{16,0},{24,8},{1,17},{9,25},{17,1},{25,9},{2,18},{10... | collective-permute-start | bytes 110600 | tf_op jit(solution)/shard_map/ppermute | solution.py:594
  65.6 23.2 %collective-permute-start = (f32[72,128]{1,0:T(8,128)S(1)}, f32[72,128]{1,0:T(8,128)S(1)}, u32[]{:S(2)}, u32[]{:S(2)}) collective-permute-start(f32[72,128]{1,0:T(8,128)S(1)} %get-tuple-element.16.refs_0_.refs_10_), channel_id=1, source_target_pairs={{0,8},{8,16},{16,24},{24,0},{1,9},{9,17},{17,25},{25,1},{2,10},{10... | collective-permute-start | bytes 110600 | tf_op jit(solution)/shard_map/ppermute | solution.py:594
  89.5 4.3 %collective-permute-start.5 = (f32[72,128]{1,0:T(8,128)S(1)}, f32[72,128]{1,0:T(8,128)S(1)}, u32[]{:S(2)}, u32[]{:S(2)}) collective-permute-start(f32[72,128]{1,0:T(8,128)S(1)} %row_state.1), channel_id=1, source_target_pairs={{0,96},{32,0},{64,32},{96,64},{1,97},{33,1},{65,33},{97,65},{2,98}... | collective-permute-start | bytes 110600 | tf_op jit(solution)/shard_map/ppermute | solution.py:594
  92.8 4.4 %collective-permute-start.4 = (f32[72,128]{1,0:T(8,128)S(1)}, f32[72,128]{1,0:T(8,128)S(1)}, u32[]{:S(2)}, u32[]{:S(2)}) collective-permute-start(f32[72,128]{1,0:T(8,128)S(1)} %row_state.1), channel_id=1, source_target_pairs={{0,64},{32,96},{64,0},{96,32},{1,65},{33,97},{65,1},{97,33},{2,66}... | collective-permute-start | bytes 110600 | tf_op jit(solution)/shard_map/ppermute | solution.py:594
  92.9 4.4 %collective-permute-start.3 = (f32[72,128]{1,0:T(8,128)S(1)}, f32[72,128]{1,0:T(8,128)S(1)}, u32[]{:S(2)}, u32[]{:S(2)}) collective-permute-start(f32[72,128]{1,0:T(8,128)S(1)} %row_state.1), channel_id=1, source_target_pairs={{0,32},{32,64},{64,96},{96,0},{1,33},{33,65},{65,97},{97,1},{2,34}... | collective-permute-start | bytes 110600 | tf_op jit(solution)/shard_map/ppermute | solution.py:594
  104.9 14.4 %collective-permute-start.6 = (bf16[272,128]{1,0:T(8,128)(2,1)S(1)}, bf16[272,128]{1,0:T(8,128)(2,1)S(1)}, u32[]{:S(2)}, u32[]{:S(2)}) collective-permute-start(bf16[272,128]{1,0:T(8,128)(2,1)S(1)} %get-tuple-element.18), channel_id=1, source_target_pairs={{0,1},{1,2},{2,3},{3,4},{4,5},{5,6},{6,7},{7,0},{8,9},{9,10},{10,1... | collective-permute-start | bytes 208904 | tf_op jit(solution)/shard_map/ppermute | solution.py:594
  108.9 11.3 %collective-permute-start.7 = (bf16[272,128]{1,0:T(8,128)(2,1)S(1)}, bf16[272,128]{1,0:T(8,128)(2,1)S(1)}, u32[]{:S(2)}, u32[]{:S(2)}) collective-permute-start(bf16[272,128]{1,0:T(8,128)(2,1)S(1)} %get-tuple-element.19), channel_id=1, source_target_pairs={{0,2},{1,3},{2,4},{3,5},{4,6},{5,7},{6,0},{7,1},{8,10},{9,11},{10,... | collective-permute-start | bytes 208904 | tf_op jit(solution)/shard_map/ppermute | solution.py:594
  110.1 11.7 %copy-start = (s32[8,192]{1,0:T(8,128)S(1)}, s32[8,192]{1,0:T(8,128)}, u32[]{:S(2)}) copy-start(s32[8,192]{1,0:T(8,128)} %get-tuple-element.26.refs_1_) | copy-start | bytes 18436
  110.1 11.7 %copy-start.1 = (f32[192,2]{0,1:T(2,128)S(1)}, f32[192,2]{0,1:T(2,128)}, u32[]{:S(2)}) copy-start(f32[192,2]{0,1:T(2,128)} %param.33) | copy-start | bytes 4612
  115.4 9.7 %collective-permute-start.8 = (bf16[272,128]{1,0:T(8,128)(2,1)S(1)}, bf16[272,128]{1,0:T(8,128)(2,1)S(1)}, u32[]{:S(2)}, u32[]{:S(2)}) collective-permute-start(bf16[272,128]{1,0:T(8,128)(2,1)S(1)} %get-tuple-element.20), channel_id=1, source_target_pairs={{0,3},{1,4},{2,5},{3,6},{4,7},{5,0},{6,1},{7,2},{8,11},{9,12},{10,... | collective-permute-start | bytes 208904 | tf_op jit(solution)/shard_map/ppermute | solution.py:594
  117.0 8.1 %collective-permute-start.9 = (bf16[272,128]{1,0:T(8,128)(2,1)S(1)}, bf16[272,128]{1,0:T(8,128)(2,1)S(1)}, u32[]{:S(2)}, u32[]{:S(2)}) collective-permute-start(bf16[272,128]{1,0:T(8,128)(2,1)S(1)} %get-tuple-element.21), channel_id=1, source_target_pairs={{0,4},{1,5},{2,6},{3,7},{4,0},{5,1},{6,2},{7,3},{8,12},{9,13},{10,... | collective-permute-start | bytes 208904 | tf_op jit(solution)/shard_map/ppermute | solution.py:594
  117.5 7.6 %collective-permute-start.10 = (bf16[272,128]{1,0:T(8,128)(2,1)S(1)}, bf16[272,128]{1,0:T(8,128)(2,1)S(1)}, u32[]{:S(2)}, u32[]{:S(2)}) collective-permute-start(bf16[272,128]{1,0:T(8,128)(2,1)S(1)} %get-tuple-element.22), channel_id=1, source_target_pairs={{0,5},{1,6},{2,7},{3,0},{4,1},{5,2},{6,3},{7,4},{8,13},{9,14},{10,... | collective-permute-start | bytes 208904 | tf_op jit(solution)/shard_map/ppermute | solution.py:594
  119.4 5.7 %collective-permute-start.11 = (bf16[272,128]{1,0:T(8,128)(2,1)S(1)}, bf16[272,128]{1,0:T(8,128)(2,1)S(1)}, u32[]{:S(2)}, u32[]{:S(2)}) collective-permute-start(bf16[272,128]{1,0:T(8,128)(2,1)S(1)} %get-tuple-element.23), channel_id=1, source_target_pairs={{0,6},{1,7},{2,0},{3,1},{4,2},{5,3},{6,4},{7,5},{8,14},{9,15},{10,... | collective-permute-start | bytes 208904 | tf_op jit(solution)/shard_map/ppermute | solution.py:594
  120.2 4.9 %collective-permute-start.12 = (bf16[272,128]{1,0:T(8,128)(2,1)S(1)}, bf16[272,128]{1,0:T(8,128)(2,1)S(1)}, u32[]{:S(2)}, u32[]{:S(2)}) collective-permute-start(bf16[272,128]{1,0:T(8,128)(2,1)S(1)} %get-tuple-element.24), channel_id=1, source_target_pairs={{0,7},{1,0},{2,1},{3,2},{4,3},{5,4},{6,5},{7,6},{8,15},{9,8},{10,9... | collective-permute-start | bytes 208904 | tf_op jit(solution)/shard_map/ppermute | solution.py:594

commit v4 on v3

--- a/solution.py
+++ b/solution.py
@@ -111,7 +111,7 @@
 
 def start(x, gain, idx, keys, values, in_gate, forget, extra, bias, cap, experts):
     tokens, width = x.shape
-    pieces = 4
+    pieces = 2
     shape = (pieces, experts // (2 * pieces), 2, 2 * cap, width // 2)
     inputs = (idx, gain, in_gate, forget, extra, keys, values, x)
     hbm = pl.BlockSpec(memory_space=pltpu.HBM)
@@ -286,16 +286,19 @@
     weight_col = jnp.transpose(jnp.concatenate([weight_ref[...]] * 4, axis=0)).astype(BF16)
     lane = iota((tokens, total), 1)
     at = [(s // cap) * (2 * cap) + s % cap for s in (slot_col[:, 0:1], slot_col[:, 1:2])]
-    for h in range(2):
-        cols = slice(h * half, (h + 1) * half)
-        mix = jnp.where(
+    mix = [
+        jnp.where(
             lane == at[0] + h * cap,
             weight_col[:, 0:1].astype(F32),
             jnp.where(lane == at[1] + h * cap, weight_col[:, 1:2].astype(F32), 0.0),
         ).astype(BF16)
-        routed = dot(mix, back_ref[...])
+        for h in range(2)
+    ]
+    routed = dot(jnp.concatenate(mix, axis=0), back_ref[...])
+    for h in range(2):
+        cols = slice(h * half, (h + 1) * half)
         loads[h].wait()
-        out_ref[:, cols] = (routed + shared_ref[:, cols]).astype(BF16)
+        out_ref[:, cols] = (routed[h * tokens : (h + 1) * tokens] + shared_ref[:, cols]).astype(BF16)
         stores[h].start()
     for store in stores:
         store.wait()

time: 128 us -> 129 us (level)
  no operation moved by 1% of the time
where the time goes in v4:
time: 129 us; the launch traced here: 128 us
  blocking collectives  41.6 us (32%)
  Pallas kernels  34.6 us (27%)
  waiting for transfers between devices  26.2 us (20%)
  starting transfers between devices  24.3 us (19%)
  between operations  1.54 us (1%)
    all_to_all x1, blocking collectives, exchange(): return lax.all_to_all(x, axes, split_axis=0, concat_axis=0, tiled=True)  41.6 us
    ppermute x13, waiting for transfers between devices, from_earlier(): lax.ppermute(shard, axis, [(p, (p + k) % count) for p in range(count)])  26.2 us
    ppermute x13, starting transfers between devices, from_earlier(): lax.ppermute(shard, axis, [(p, (p + k) % count) for p in range(count)])  19.6 us
    pallas_call x1, Pallas kernels, expert_products(): pl.pallas_call(body, in_specs=[pl.BlockSpec(memory_space=pltpu.VMEM), hbm...  10.1 us
    pallas_call x1, Pallas kernels, mixer_rows(): pl.pallas_call(body, in_specs=[smem, smem] + [vmem] * (8 + len(rows) + le...  7.59 us
    pallas_call x1, Pallas kernels, shared_expert(): pl.pallas_call(shared_body, out_shape=pltpu.HBM((tokens, width), F32), co...  5.25 us
    all_to_all x1, starting transfers between devices, exchange(): return lax.all_to_all(x, axes, split_axis=0, concat_axis=0, tiled=True)  4.76 us
    pallas_call x1, Pallas kernels, start(): pl.pallas_call(body, in_specs=[pl.BlockSpec(memory_space=pltpu.SMEM)] + [...  4.65 us
  transfers between devices with their start and end apart: 14, of which 6 were waited for; matrix products, arithmetic and copies ran while one was open for 0% of the time, Pallas kernels for 13%

profile of v4, /device:TPU:1, one launch (start us, length us, event | category | flops | bytes accessed | tf_op | source)
XLA Modules:
  0.0 128.3 jit_solution(9382017396563057517)
XLA Ops:
  1.3 4.6 %start.1 = (bf16[2,32,2,8,1024]{4,3,2,1,0:T(8,128)(2,1)}, bf16[192,2048]{1,0:T(8,128)(2,1)}, s32[8,192]{1,0:T(8,128)}, f32[72,128]{1,0:T(8,128)S(1)}) custom-call(f32[1]{0:T(128)S(6)} %copy.22.refs_0_.refs_1_, s32[2,192]{1,0:T(2,128)} %bitcast.30, f32[1,2048]{1,0:T(1,128)} %bitcast.23, f32[16,128]{1,0:T(8,128)} %bitcast.24, f32[16,128]{1,0:T(8,128)} %bitcast.26, ...), custom_call_target="tpu_custom_call" | custom-call | flops 402653184 | bytes 4194304 | tf_op jit(solution)/shard_map/start/pallas_call | solution.py:119
  5.9 41.6 %all_to_all.10 = bf16[128,8,1024]{2,1,0:T(8,128)(2,1)S(1)} all-to-all(bf16[128,8,1024]{2,1,0:T(8,128)(2,1)} %bitcast.20), channel_id=1, replica_groups=mesh['ep_0'=4,'ep_1'=4,'tp'=8] {'ep_0','ep_1','tp'}, dimensions={0} | all-to-all | bytes 4194304 | tf_op jit(solution)/shard_map/all_to_all | solution.py:591
  47.5 10.1 %expert_products.1 = bf16[64,2,8,1024]{3,2,1,0:T(8,128)(2,1)} custom-call(bf16[64,2,8,1024]{3,2,1,0:T(8,128)(2,1)S(1)} %bitcast.17, bf16[1,2048,1024]{2,1,0:T(8,128)(2,1)} %refs_1_.2, bf16[1,2048,1024]{2,1,0:T(8,128)(2,1)} %refs_2_.1, bf16[1,1024,2048]{2,1,0:T(8,128)(2,1)} %refs_3_.1), custom_call_target="tpu_custom_call" | custom-call | flops 6442450944 | bytes 12582912 | tf_op jit(solution)/shard_map/expert_products/pallas_call | solution.py:229
  57.6 4.8 %all-to-all-start.1 = ((bf16[128,8,1024]{2,1,0:T(8,128)(2,1)}), bf16[128,8,1024]{2,1,0:T(8,128)(2,1)S(1)}, u32[]{:S(2)}, u32[]{:S(2)}) async-start(bf16[128,8,1024]{2,1,0:T(8,128)(2,1)} %bitcast.19), calls=%async_computation.1 | async-start | bytes 4194304 | tf_op jit(solution)/shard_map/all_to_all | solution.py:591
  62.4 2.7 %collective-permute-start.2 = (f32[72,128]{1,0:T(8,128)S(1)}, f32[72,128]{1,0:T(8,128)S(1)}, u32[]{:S(2)}, u32[]{:S(2)}) collective-permute-start(f32[72,128]{1,0:T(8,128)S(1)} %get-tuple-element.16.refs_0_.refs_10_), channel_id=1, source_target_pairs={{0,24},{8,0},{16,8},{24,16},{1,25},{9,1},{17,9},{25,17},{2,26},{10... | collective-permute-start | bytes 110600 | tf_op jit(solution)/shard_map/ppermute | solution.py:597
  65.1 0.5 collective-permute-start.1
  65.6 0.6 collective-permute-start
  66.2 0.1 pad_add_fusion.place_ref.refs_0_
  66.3 20.7 %collective-permute-done.2.refs_3_.refs_13_ = f32[72,128]{1,0:T(8,128)S(1)} collective-permute-done((f32[72,128]{1,0:T(8,128)S(1)}, f32[72,128]{1,0:T(8,128)S(1)}, u32[]{:S(2)}, u32[]{:S(2)}) %collective-permute-start.2) | collective-permute-done | bytes 36896 | tf_op jit(solution)/shard_map/ppermute | solution.py:597
  87.0 1.5 %collective-permute-done.1.refs_2_.refs_12_ = f32[72,128]{1,0:T(8,128)S(1)} collective-permute-done((f32[72,128]{1,0:T(8,128)S(1)}, f32[72,128]{1,0:T(8,128)S(1)}, u32[]{:S(2)}, u32[]{:S(2)}) %collective-permute-start.1) | collective-permute-done | bytes 36896 | tf_op jit(solution)/shard_map/ppermute | solution.py:597
  88.5 0.3 collective-permute-done.refs_1_.refs_11_
  88.8 0.8 row_state.1
  89.6 3.3 %collective-permute-start.5 = (f32[72,128]{1,0:T(8,128)S(1)}, f32[72,128]{1,0:T(8,128)S(1)}, u32[]{:S(2)}, u32[]{:S(2)}) collective-permute-start(f32[72,128]{1,0:T(8,128)S(1)} %row_state.1), channel_id=1, source_target_pairs={{0,96},{32,0},{64,32},{96,64},{1,97},{33,1},{65,33},{97,65},{2,98}... | collective-permute-start | bytes 110600 | tf_op jit(solution)/shard_map/ppermute | solution.py:597
  92.9 0.1 collective-permute-start.4
  93.0 0.8 collective-permute-start.3
  93.7 0.2 collective-permute-done.5.refs_16_
  93.9 3.3 %collective-permute-done.4.refs_15_ = f32[72,128]{1,0:T(8,128)S(1)} collective-permute-done((f32[72,128]{1,0:T(8,128)S(1)}, f32[72,128]{1,0:T(8,128)S(1)}, u32[]{:S(2)}, u32[]{:S(2)}) %collective-permute-start.4) | collective-permute-done | bytes 36896 | tf_op jit(solution)/shard_map/ppermute | solution.py:597
  97.3 0.1 collective-permute-done.3.refs_14_
  97.4 7.6 %mixer_rows.1 = (bf16[272,128]{1,0:T(8,128)(2,1)S(1)}, bf16[272,128]{1,0:T(8,128)(2,1)S(1)}, bf16[272,128]{1,0:T(8,128)(2,1)S(1)}, bf16[272,128]{1,0:T(8,128)(2,...) custom-call(s32[3]{0:T(128)S(1)} %pad_add_fusion.place_ref.refs_0_, ...), custom_call_target="tpu_custom_call" | custom-call | flops 1073741824 | bytes 2097152 | tf_op jit(solution)/shard_map/mixer_rows/pallas_call | solution.py:522
  105.0 3.9 %collective-permute-start.6 = (bf16[272,128]{1,0:T(8,128)(2,1)S(1)}, bf16[272,128]{1,0:T(8,128)(2,1)S(1)}, u32[]{:S(2)}, u32[]{:S(2)}) collective-permute-start(bf16[272,128]{1,0:T(8,128)(2,1)S(1)} %get-tuple-element.18), channel_id=1, source_target_pairs={{0,1},{1,2},{2,3},{3,4},{4,5},{5,6},{6,7},{7,0},{8,9},{9,10},{10,1... | collective-permute-start | bytes 208904 | tf_op jit(solution)/shard_map/ppermute | solution.py:597
  108.9 1.2 collective-permute-start.7
  110.2 5.2 %shared_expert.1.refs_3_ = f32[192,2048]{1,0:T(8,128)} custom-call(bf16[192,2048]{1,0:T(8,128)(2,1)} %get-tuple-element.27.n_ref, bf16[2048,384]{1,0:T(8,128)(2,1)} %g_ref.1, bf16[2048,384]{1,0:T(8,128)(2,1)} %u_ref.1, bf16[384,2048]{1,0:T(8,128)(2,1)} %d_ref.1), custom_call_target="tpu_custom_call" | custom-call | flops 905969664 | bytes 4718592 | tf_op jit(solution)/shard_map/shared_expert/pallas_call | solution.py:261
  115.4 1.6 %collective-permute-start.8 = (bf16[272,128]{1,0:T(8,128)(2,1)S(1)}, bf16[272,128]{1,0:T(8,128)(2,1)S(1)}, u32[]{:S(2)}, u32[]{:S(2)}) collective-permute-start(bf16[272,128]{1,0:T(8,128)(2,1)S(1)} %get-tuple-element.20), channel_id=1, source_target_pairs={{0,3},{1,4},{2,5},{3,6},{4,7},{5,0},{6,1},{7,2},{8,11},{9,12},{10,... | collective-permute-start | bytes 208904 | tf_op jit(solution)/shard_map/ppermute | solution.py:597
  117.1 0.4 collective-permute-start.9
  117.5 1.9 %collective-permute-start.10 = (bf16[272,128]{1,0:T(8,128)(2,1)S(1)}, bf16[272,128]{1,0:T(8,128)(2,1)S(1)}, u32[]{:S(2)}, u32[]{:S(2)}) collective-permute-start(bf16[272,128]{1,0:T(8,128)(2,1)S(1)} %get-tuple-element.22), channel_id=1, source_target_pairs={{0,5},{1,6},{2,7},{3,0},{4,1},{5,2},{6,3},{7,4},{8,13},{9,14},{10,... | collective-permute-start | bytes 208904 | tf_op jit(solution)/shard_map/ppermute | solution.py:597
  119.4 0.0 collective-permute-done.6.refs_2_
  119.4 0.8 collective-permute-start.11
  120.2 0.0 collective-permute-done.7.refs_3_
  120.2 1.6 %collective-permute-start.12 = (bf16[272,128]{1,0:T(8,128)(2,1)S(1)}, bf16[272,128]{1,0:T(8,128)(2,1)S(1)}, u32[]{:S(2)}, u32[]{:S(2)}) collective-permute-start(bf16[272,128]{1,0:T(8,128)(2,1)S(1)} %get-tuple-element.24), channel_id=1, source_target_pairs={{0,7},{1,0},{2,1},{3,2},{4,3},{5,4},{6,5},{7,6},{8,15},{9,8},{10,9... | collective-permute-start | bytes 208904 | tf_op jit(solution)/shard_map/ppermute | solution.py:597
  121.8 0.0 all-to-all-done.1
  121.8 3.7 %combine.1 = (bf16[192,2048]{1,0:T(8,128)(2,1)}, bf16[1024,2048]{1,0:T(8,128)(2,1)S(1)}) custom-call(bf16[1024,1024]{1,0:T(8,128)(2,1)S(1)} %bitcast.16, s32[8,192]{1,0:T(8,128)S(1)} %copy-done, f32[2,192]{1,0:T(2,128)S(1)} %bitcast.18, f32[192,2048]{1,0:T(8,128)} %shared_expert.1.refs_3_, bf16[1024,2048]{1,0:T(8,128)(2,1)} %refs_4_.3), custom_call_target="tpu_custom_call" | custom-call | flops 1610612736 | bytes 2097152 | tf_op jit(solution)/shard_map/combine/pallas_call | solution.py:313
  125.6 2.6 %project.1 = bf16[256,2048]{1,0:T(8,128)(2,1)} custom-call(s32[3]{0:T(128)S(1)} %pad_add_fusion.place_ref.refs_0_, bf16[272,128]{1,0:T(8,128)(2,1)S(1)} %get-tuple-element.17.refs_1_, bf16[272,128]{1,0:T(8,128)(2,1)S(1)} %collective-permute-done.6.refs_2_, bf16[272,128]{1,0:T(8,128)(2,1)S(1)} %collective-permute-done.7.refs_3_, ...), custom_call_target="tpu_custom_call" | custom-call | flops 1073741824 | bytes 4194304 | tf_op jit(solution)/shard_map/project/pallas_call | solution.py:574
  (9 shorter events, 0.0 us)
Async XLA Ops:
  57.6 64.2 %all-to-all-start.1 = ((bf16[128,8,1024]{2,1,0:T(8,128)(2,1)}), bf16[128,8,1024]{2,1,0:T(8,128)(2,1)S(1)}, u32[]{:S(2)}, u32[]{:S(2)}) async-start(bf16[128,8,1024]{2,1,0:T(8,128)(2,1)} %bitcast.19), calls=%async_computation.1 | async-start | bytes 4194304 | tf_op jit(solution)/shard_map/all_to_all | solution.py:591
  62.4 24.6 %collective-permute-start.2 = (f32[72,128]{1,0:T(8,128)S(1)}, f32[72,128]{1,0:T(8,128)S(1)}, u32[]{:S(2)}, u32[]{:S(2)}) collective-permute-start(f32[72,128]{1,0:T(8,128)S(1)} %get-tuple-element.16.refs_0_.refs_10_), channel_id=1, source_target_pairs={{0,24},{8,0},{16,8},{24,16},{1,25},{9,1},{17,9},{25,17},{2,26},{10... | collective-permute-start | bytes 110600 | tf_op jit(solution)/shard_map/ppermute | solution.py:597
  65.1 23.5 %collective-permute-start.1 = (f32[72,128]{1,0:T(8,128)S(1)}, f32[72,128]{1,0:T(8,128)S(1)}, u32[]{:S(2)}, u32[]{:S(2)}) collective-permute-start(f32[72,128]{1,0:T(8,128)S(1)} %get-tuple-element.16.refs_0_.refs_10_), channel_id=1, source_target_pairs={{0,16},{8,24},{16,0},{24,8},{1,17},{9,25},{17,1},{25,9},{2,18},{10... | collective-permute-start | bytes 110600 | tf_op jit(solution)/shard_map/ppermute | solution.py:597
  65.6 23.2 %collective-permute-start = (f32[72,128]{1,0:T(8,128)S(1)}, f32[72,128]{1,0:T(8,128)S(1)}, u32[]{:S(2)}, u32[]{:S(2)}) collective-permute-start(f32[72,128]{1,0:T(8,128)S(1)} %get-tuple-element.16.refs_0_.refs_10_), channel_id=1, source_target_pairs={{0,8},{8,16},{16,24},{24,0},{1,9},{9,17},{17,25},{25,1},{2,10},{10... | collective-permute-start | bytes 110600 | tf_op jit(solution)/shard_map/ppermute | solution.py:597
  89.6 4.3 %collective-permute-start.5 = (f32[72,128]{1,0:T(8,128)S(1)}, f32[72,128]{1,0:T(8,128)S(1)}, u32[]{:S(2)}, u32[]{:S(2)}) collective-permute-start(f32[72,128]{1,0:T(8,128)S(1)} %row_state.1), channel_id=1, source_target_pairs={{0,96},{32,0},{64,32},{96,64},{1,97},{33,1},{65,33},{97,65},{2,98}... | collective-permute-start | bytes 110600 | tf_op jit(solution)/shard_map/ppermute | solution.py:597
  92.9 4.4 %collective-permute-start.4 = (f32[72,128]{1,0:T(8,128)S(1)}, f32[72,128]{1,0:T(8,128)S(1)}, u32[]{:S(2)}, u32[]{:S(2)}) collective-permute-start(f32[72,128]{1,0:T(8,128)S(1)} %row_state.1), channel_id=1, source_target_pairs={{0,64},{32,96},{64,0},{96,32},{1,65},{33,97},{65,1},{97,33},{2,66}... | collective-permute-start | bytes 110600 | tf_op jit(solution)/shard_map/ppermute | solution.py:597
  93.0 4.4 %collective-permute-start.3 = (f32[72,128]{1,0:T(8,128)S(1)}, f32[72,128]{1,0:T(8,128)S(1)}, u32[]{:S(2)}, u32[]{:S(2)}) collective-permute-start(f32[72,128]{1,0:T(8,128)S(1)} %row_state.1), channel_id=1, source_target_pairs={{0,32},{32,64},{64,96},{96,0},{1,33},{33,65},{65,97},{97,1},{2,34}... | collective-permute-start | bytes 110600 | tf_op jit(solution)/shard_map/ppermute | solution.py:597
  105.0 14.4 %collective-permute-start.6 = (bf16[272,128]{1,0:T(8,128)(2,1)S(1)}, bf16[272,128]{1,0:T(8,128)(2,1)S(1)}, u32[]{:S(2)}, u32[]{:S(2)}) collective-permute-start(bf16[272,128]{1,0:T(8,128)(2,1)S(1)} %get-tuple-element.18), channel_id=1, source_target_pairs={{0,1},{1,2},{2,3},{3,4},{4,5},{5,6},{6,7},{7,0},{8,9},{9,10},{10,1... | collective-permute-start | bytes 208904 | tf_op jit(solution)/shard_map/ppermute | solution.py:597
  108.9 11.3 %collective-permute-start.7 = (bf16[272,128]{1,0:T(8,128)(2,1)S(1)}, bf16[272,128]{1,0:T(8,128)(2,1)S(1)}, u32[]{:S(2)}, u32[]{:S(2)}) collective-permute-start(bf16[272,128]{1,0:T(8,128)(2,1)S(1)} %get-tuple-element.19), channel_id=1, source_target_pairs={{0,2},{1,3},{2,4},{3,5},{4,6},{5,7},{6,0},{7,1},{8,10},{9,11},{10,... | collective-permute-start | bytes 208904 | tf_op jit(solution)/shard_map/ppermute | solution.py:597
  110.2 11.7 %copy-start = (s32[8,192]{1,0:T(8,128)S(1)}, s32[8,192]{1,0:T(8,128)}, u32[]{:S(2)}) copy-start(s32[8,192]{1,0:T(8,128)} %get-tuple-element.26.refs_1_) | copy-start | bytes 18436
  110.2 11.7 %copy-start.1 = (f32[192,2]{0,1:T(2,128)S(1)}, f32[192,2]{0,1:T(2,128)}, u32[]{:S(2)}) copy-start(f32[192,2]{0,1:T(2,128)} %param.33) | copy-start | bytes 4612
  115.4 10.1 %collective-permute-start.8 = (bf16[272,128]{1,0:T(8,128)(2,1)S(1)}, bf16[272,128]{1,0:T(8,128)(2,1)S(1)}, u32[]{:S(2)}, u32[]{:S(2)}) collective-permute-start(bf16[272,128]{1,0:T(8,128)(2,1)S(1)} %get-tuple-element.20), channel_id=1, source_target_pairs={{0,3},{1,4},{2,5},{3,6},{4,7},{5,0},{6,1},{7,2},{8,11},{9,12},{10,... | collective-permute-start | bytes 208904 | tf_op jit(solution)/shard_map/ppermute | solution.py:597
  117.1 8.5 %collective-permute-start.9 = (bf16[272,128]{1,0:T(8,128)(2,1)S(1)}, bf16[272,128]{1,0:T(8,128)(2,1)S(1)}, u32[]{:S(2)}, u32[]{:S(2)}) collective-permute-start(bf16[272,128]{1,0:T(8,128)(2,1)S(1)} %get-tuple-element.21), channel_id=1, source_target_pairs={{0,4},{1,5},{2,6},{3,7},{4,0},{5,1},{6,2},{7,3},{8,12},{9,13},{10,... | collective-permute-start | bytes 208904 | tf_op jit(solution)/shard_map/ppermute | solution.py:597
  117.5 8.1 %collective-permute-start.10 = (bf16[272,128]{1,0:T(8,128)(2,1)S(1)}, bf16[272,128]{1,0:T(8,128)(2,1)S(1)}, u32[]{:S(2)}, u32[]{:S(2)}) collective-permute-start(bf16[272,128]{1,0:T(8,128)(2,1)S(1)} %get-tuple-element.22), channel_id=1, source_target_pairs={{0,5},{1,6},{2,7},{3,0},{4,1},{5,2},{6,3},{7,4},{8,13},{9,14},{10,... | collective-permute-start | bytes 208904 | tf_op jit(solution)/shard_map/ppermute | solution.py:597
  119.4 6.2 %collective-permute-start.11 = (bf16[272,128]{1,0:T(8,128)(2,1)S(1)}, bf16[272,128]{1,0:T(8,128)(2,1)S(1)}, u32[]{:S(2)}, u32[]{:S(2)}) collective-permute-start(bf16[272,128]{1,0:T(8,128)(2,1)S(1)} %get-tuple-element.23), channel_id=1, source_target_pairs={{0,6},{1,7},{2,0},{3,1},{4,2},{5,3},{6,4},{7,5},{8,14},{9,15},{10,... | collective-permute-start | bytes 208904 | tf_op jit(solution)/shard_map/ppermute | solution.py:597
  120.2 5.4 %collective-permute-start.12 = (bf16[272,128]{1,0:T(8,128)(2,1)S(1)}, bf16[272,128]{1,0:T(8,128)(2,1)S(1)}, u32[]{:S(2)}, u32[]{:S(2)}) collective-permute-start(bf16[272,128]{1,0:T(8,128)(2,1)S(1)} %get-tuple-element.24), channel_id=1, source_target_pairs={{0,7},{1,0},{2,1},{3,2},{4,3},{5,4},{6,5},{7,6},{8,15},{9,8},{10,9... | collective-permute-start | bytes 208904 | tf_op jit(solution)/shard_map/ppermute | solution.py:597
